TPU v7x, 512 devices: a whole 4x8x8 slice. The times are simulated.
512 devices in a mesh: sp: 64 (over z, y), dp: 8 (over x, core).
Axes of the slice: x: 4, y: 8, z: 8, core: 2. Of those that a mesh axis runs over, the one named last changes fastest.
Arguments:
- gated: bfloat16 [8, 8192, 3072], P('dp', 'sp'), may hold values from -6 to 6
- values_in: bfloat16 [8, 8192, 3072], P('dp', 'sp'), may hold values from -6 to 6
- upstream: bfloat16 [8, 8192, 3072], P('dp', 'sp'), may hold values from -6 to 6
- gain: float32 [3072], replicated, may hold values from 0.1 to 1.9
- shift: float32 [3072], replicated, may hold values from -3 to 3
- mix_w: bfloat16 [512, 4, 512], P('dp'), may hold values from -0.375 to 0.375
- mix_bias: float32 [4, 512], replicated, may hold values from 0.1 to 1.9
Outputs:
- grad_u: bfloat16 [8, 8192, 3072], P('dp', 'sp')
- grad_v: bfloat16 [8, 8192, 3072], P('dp', 'sp')
- grad_mix: float32 [512, 4, 512], P('dp')
- grad_bias: float32 [4, 512], replicated
- grad_gain: float32 [3072], replicated
- grad_shift: float32 [3072], replicated
All inputs are finite; a program needn't handle non-finite values.
Results may differ from a plain program's by a relative error of at most 0.014.
Values may be sent and summed in bfloat16 or wider, within the bound.
A program may use at most 64 MiB of HBM per device.

v0:
```python
import jax
import jax.numpy as jnp
from jax import lax
from jax.sharding import Mesh
from jax.sharding import PartitionSpec as P

SEG = 64
DP = ("dp_0", "dp_1")
SP = ("sp_0", "sp_1")
SP_DP = ("sp_0", "sp_1", "dp_0", "dp_1")


EPS = 1e-05


def joined_along(pieces, dim):
    pieces = jnp.moveaxis(pieces, 0, dim)
    dims = pieces.shape
    return pieces.reshape(*dims[:dim], dims[dim] * dims[dim + 1], *dims[dim + 2 :])


def sent_to_all(x, axis):
    copies = jnp.broadcast_to(x, (lax.axis_size(axis), *x.shape))
    return lax.all_to_all(copies, axis, split_axis=0, concat_axis=0, tiled=True)


def gather_directly(x, axis, dim):
    return joined_along(sent_to_all(x, axis), dim)


def cut_along(x, dim, devices):
    before, after = (x.shape[:dim], x.shape[dim + 1 :])
    return jnp.moveaxis(x.reshape(*before, devices, -1, *after), dim, 0)


def sum_at_owner(x, axis, dim):
    pieces = cut_along(x, dim, lax.axis_size(axis))
    arrived = lax.all_to_all(pieces, axis, split_axis=0, concat_axis=0, tiled=True)
    return arrived.astype(jnp.float32).sum(axis=0)


def sum_at_owner_2(x, axis, dim):
    devices = lax.axis_size(axis)
    pieces = lax.all_to_all(cut_along(x, dim, devices), axis, 0, 0, tiled=True)
    return jnp.sum(pieces, axis=0)


def by_axis(x, axes):
    for axis in axes:
        x = lax.psum(x, axis)
    return x


def span_allowed(span_len):
    places = jnp.arange(span_len)
    return places[:, None] // SEG >= places[None, :] // SEG


def by_groups(normed, mix_grad, mix_w, mix_bias):
    tok_rows, half_width = normed.shape
    dp_count = lax.axis_size(DP)
    sp_count = lax.axis_size(SP)
    span_len, groups = (mix_w.shape[0] * dp_count, mix_w.shape[1])
    group_width = half_width // groups
    channels = half_width // sp_count
    my_group = lax.axis_index(SP) * channels // group_width
    own_rows = lax.dynamic_index_in_dim(mix_w, my_group, 1, keepdims=False)
    gathered = gather_directly(own_rows, DP, 0)
    allowed = span_allowed(span_len)
    weights = jnp.where(allowed, gathered, jnp.zeros_like(gathered))
    sent_norm, sent_grad = (
        lax.all_to_all(normed.T, SP, split_axis=0, concat_axis=1, tiled=True),
        lax.all_to_all(mix_grad.T, SP, split_axis=0, concat_axis=1, tiled=True),
    )
    seq_len = sent_norm.shape[1]
    blocks = seq_len // span_len
    norm_blocks = sent_norm.reshape(channels, blocks, span_len)
    grad_blocks = sent_grad.reshape(channels, blocks, span_len)
    bias_row = lax.dynamic_index_in_dim(mix_bias, my_group, 0, keepdims=False)
    mixed_f = (
        jnp.einsum("ts,cns->cnt", weights, norm_blocks, preferred_element_type=jnp.float32)
        + bias_row[None, None, :]
    )
    mixed_b = lax.optimization_barrier(mixed_f.astype(jnp.bfloat16))
    back_f = jnp.einsum("ts,cnt->cns", weights, grad_blocks, preferred_element_type=jnp.float32)
    back_b = lax.optimization_barrier(back_f.astype(jnp.bfloat16))
    mixed_tok, back_tok = (
        lax.all_to_all(
            mixed_b.reshape(channels, seq_len), SP, split_axis=1, concat_axis=0, tiled=True
        ),
        lax.all_to_all(
            back_b.reshape(channels, seq_len), SP, split_axis=1, concat_axis=0, tiled=True
        ),
    )
    group_term = jnp.einsum(
        "cnt,cns->ts", grad_blocks, norm_blocks, preferred_element_type=jnp.float32
    )
    group_term = group_term * allowed.astype(jnp.float32)
    chosen = (jnp.arange(groups) == my_group).astype(jnp.float32)
    bias_term = chosen[:, None] * jnp.sum(grad_blocks, axis=(0, 1), dtype=jnp.float32)[None, :]
    partial_rows = sum_at_owner(group_term.astype(jnp.bfloat16), DP, 0)
    placed = chosen[None, :, None] * partial_rows[:, None, :]
    summed = sum_at_owner_2(placed, SP, 0)
    grad_mix = gather_directly(summed, SP, 0)
    return (mixed_tok.T, back_tok.T, grad_mix, bias_term)


def per_device(gated, values_in, upstream, gain, shift, mix_w, mix_bias):
    raw_values = values_in[0].astype(jnp.float32)
    centred = raw_values - jnp.mean(raw_values, axis=-1, keepdims=True)
    inv_std = lax.rsqrt(jnp.mean(centred * centred, axis=-1, keepdims=True) + EPS)
    unit_v = centred * inv_std
    normed = (unit_v * gain + shift).astype(jnp.bfloat16)
    upstream_f = upstream[0].astype(jnp.float32)
    mix_grad = (upstream_f * gated[0].astype(jnp.float32)).astype(jnp.bfloat16)
    mixed_b, back_b, grad_mix, bias_term = by_groups(normed, mix_grad, mix_w, mix_bias)
    grad_u = (upstream_f * mixed_b.astype(jnp.float32)).astype(jnp.bfloat16)
    grad_normed = back_b.astype(jnp.float32)
    scaled = grad_normed * gain
    grad_v = inv_std * (
        scaled
        - jnp.mean(scaled, axis=-1, keepdims=True)
        - unit_v * jnp.mean(scaled * unit_v, axis=-1, keepdims=True)
    )
    gain_term = jnp.sum(grad_normed * unit_v, axis=0)
    shift_term = jnp.sum(grad_normed, axis=0)
    bias_sum, gain_sum, shift_sum = (
        by_axis(bias_term, SP_DP),
        by_axis(gain_term, SP_DP),
        by_axis(shift_term, SP_DP),
    )
    return (
        grad_u[None],
        grad_v.astype(jnp.bfloat16)[None],
        grad_mix,
        bias_sum,
        gain_sum,
        shift_sum,
    )


def solution(mesh):
    torus = Mesh(mesh.devices.reshape(8, 8, 4, 2), ("sp_0", "sp_1", "dp_0", "dp_1"))
    return jax.shard_map(
        per_device,
        mesh=torus,
        in_specs=(
            P(DP, SP, None),
            P(DP, SP, None),
            P(DP, SP, None),
            P(),
            P(),
            P(DP, None, None),
            P(),
        ),
        out_specs=(P(DP, SP, None), P(DP, SP, None), P(DP, None, None), P(), P(), P()),
        check_vma=False,
    )
```

profile of v0, /device:TPU:1, one launch (start us, length us, event | category | flops | bytes accessed | tf_op | source)
XLA Modules:
  0.0 294.2 jit_solution(3864649874187127188)
XLA Ops:
  2.6 10.2 %all-to-all-start.1 = ((bf16[8,64,512]{2,1,0:T(8,128)(2,1)}), bf16[8,64,512]{2,1,0:T(8,128)(2,1)S(1)}, u32[]{:S(2)}, u32[]{:S(2)}) async-start(bf16[8,64,512]{2,1,0:T(8,128)(2,1)} %broadcast_in_dim.10), calls=%async_computation.1 | async-start | bytes 1048576 | tf_op jit(solution)/shard_map/all_to_all | solution.py:24
  15.4 6.8 %all-to-all-done.1 = bf16[8,64,512]{2,1,0:T(8,128)(2,1)S(1)} async-done(((bf16[8,64,512]{2,1,0:T(8,128)(2,1)}), bf16[8,64,512]{2,1,0:T(8,128)(2,1)S(1)}, u32[]{:S(2)}, u32[]{:S(2)}) %all-to-all-start.1) | async-done | bytes 524320 | tf_op jit(solution)/shard_map/all_to_all | solution.py:24
  22.2 11.8 %all-to-all-start.3 = ((bf16[64,48,128]{2,1,0:T(8,128)(2,1)}), bf16[64,48,128]{2,1,0:T(8,128)(2,1)S(1)}, u32[]{:S(2)}, u32[]{:S(2)}) async-start(bf16[64,48,128]{2,1,0:T(8,128)(2,1)} %bitcast.16), calls=%async_computation.3 | async-start | bytes 1572864 | tf_op jit(solution)/shard_map/all_to_all | solution.py:73
  35.1 20.4 %all-to-all-done.3 = bf16[64,48,128]{2,1,0:T(8,128)(2,1)S(1)} async-done(((bf16[64,48,128]{2,1,0:T(8,128)(2,1)}), bf16[64,48,128]{2,1,0:T(8,128)(2,1)S(1)}, u32[]{:S(2)}, u32[]{:S(2)}) %all-to-all-start.3) | async-done | bytes 786464 | tf_op jit(solution)/shard_map/all_to_all | solution.py:73
  56.2 2.8 convolution_convert_fusion
  59.0 1.6 all_to_all.65
  61.9 8.0 %all-to-all-start.4 = ((bf16[48,64,128]{2,0,1:T(8,128)(2,1)}), bf16[48,64,128]{2,0,1:T(8,128)(2,1)S(1)}, u32[]{:S(2)}, u32[]{:S(2)}) async-start(bf16[48,64,128]{2,0,1:T(8,128)(2,1)} %copy.58), calls=%async_computation.4 | async-start | bytes 1572864 | tf_op jit(solution)/shard_map/all_to_all | solution.py:91
  72.3 18.5 %all-to-all-done.4 = bf16[48,64,128]{2,0,1:T(8,128)(2,1)S(1)} async-done(((bf16[48,64,128]{2,0,1:T(8,128)(2,1)}), bf16[48,64,128]{2,0,1:T(8,128)(2,1)S(1)}, u32[]{:S(2)}, u32[]{:S(2)}) %all-to-all-start.4) | async-done | bytes 786464 | tf_op jit(solution)/shard_map/all_to_all | solution.py:91
  91.8 2.4 fusion.12
  94.2 27.6 %all_to_all.78 = bf16[64,48,128]{2,1,0:T(8,128)(2,1)S(1)} all-to-all(bf16[64,48,128]{2,1,0:T(8,128)(2,1)S(1)} %bitcast.98), channel_id=1, replica_groups=mesh['sp_0'=8,'sp_1'=8,'dp_0'=4,'dp_1'=2] {'sp_0','sp_1'}, dimensions={0} | all-to-all | bytes 1572864 | tf_op jit(solution)/shard_map/all_to_all | solution.py:72
  123.4 2.8 fusion.21
  126.1 8.9 %all-to-all-start.5 = ((bf16[8,64,512]{2,1,0:T(8,128)(2,1)}), bf16[8,64,512]{2,1,0:T(8,128)(2,1)S(1)}, u32[]{:S(2)}, u32[]{:S(2)}) async-start(bf16[8,64,512]{2,1,0:T(8,128)(2,1)} %bitcast.102), calls=%async_computation.5 | async-start | bytes 1048576 | tf_op jit(solution)/shard_map/all_to_all | solution.py:38
  135.1 9.4 %all-to-all-done.5 = bf16[8,64,512]{2,1,0:T(8,128)(2,1)S(1)} async-done(((bf16[8,64,512]{2,1,0:T(8,128)(2,1)}), bf16[8,64,512]{2,1,0:T(8,128)(2,1)S(1)}, u32[]{:S(2)}, u32[]{:S(2)}) %all-to-all-start.5) | async-done | bytes 524320 | tf_op jit(solution)/shard_map/all_to_all | solution.py:38
  145.5 6.2 %all-to-all-start.6 = ((f32[64,1,4,512]{3,2,1,0:T(4,128)}), f32[64,1,4,512]{3,2,1,0:T(4,128)}, u32[]{:S(2)}, u32[]{:S(2)}) async-start(f32[64,1,4,512]{3,2,1,0:T(4,128)} %broadcast_multiply_fusion), calls=%async_computation.6 | async-start | bytes 1048576 | tf_op jit(solution)/shard_map/all_to_all | solution.py:44
  152.4 2.5 add_convert_fusion
  157.9 10.3 %all-to-all-done.6 = f32[64,1,4,512]{3,2,1,0:T(4,128)} async-done(((f32[64,1,4,512]{3,2,1,0:T(4,128)}), f32[64,1,4,512]{3,2,1,0:T(4,128)}, u32[]{:S(2)}, u32[]{:S(2)}) %all-to-all-start.6) | async-done | bytes 524320 | tf_op jit(solution)/shard_map/all_to_all | solution.py:44
  168.2 7.0 %all-to-all-start.2 = ((bf16[48,64,128]{2,0,1:T(8,128)(2,1)}), bf16[48,64,128]{2,0,1:T(8,128)(2,1)S(1)}, u32[]{:S(2)}, u32[]{:S(2)}) async-start(bf16[48,64,128]{2,0,1:T(8,128)(2,1)} %copy.55), calls=%async_computation.2 | async-start | bytes 1572864 | tf_op jit(solution)/shard_map/all_to_all | solution.py:88
  176.6 19.6 %all-to-all-done.2 = bf16[48,64,128]{2,0,1:T(8,128)(2,1)S(1)} async-done(((bf16[48,64,128]{2,0,1:T(8,128)(2,1)}), bf16[48,64,128]{2,0,1:T(8,128)(2,1)S(1)}, u32[]{:S(2)}, u32[]{:S(2)}) %all-to-all-start.2) | async-done | bytes 786464 | tf_op jit(solution)/shard_map/all_to_all | solution.py:88
  197.0 8.5 %all-to-all-start.7 = ((f32[64,1,4,512]{3,2,1,0:T(4,128)}), f32[64,1,4,512]{3,2,1,0:T(4,128)}, u32[]{:S(2)}, u32[]{:S(2)}) async-start(f32[64,1,4,512]{3,2,1,0:T(4,128)} %broadcast_in_dim.14), calls=%async_computation.7 | async-start | bytes 1048576 | tf_op jit(solution)/shard_map/all_to_all | solution.py:24
  207.4 27.1 %all-reduce.1 = (f32[4,512]{1,0:T(4,128)S(1)}, f32[3072]{0:T(1024)S(1)}, f32[3072]{0:T(1024)S(1)}) all-reduce(f32[4,512]{1,0:T(4,128)S(1)} %broadcast_multiply_fusion.1, f32[3072]{0:T(1024)S(1)} %get-tuple-element.30, f32[3072]{0:T(1024)S(1)} %reduce_sum.101), channel_id=1, replica_groups=mesh['sp_0'=8,'sp_1'=8,'dp_0'=4,'dp_1'=2] {'sp_0'}, use_global_device_ids=true, to_apply=%region_8.9 | all-reduce | flops 8192 | bytes 65536 | tf_op jit(solution)/shard_map/psum | solution.py:50
  234.4 23.3 %all-reduce = (f32[4,512]{1,0:T(4,128)S(1)}, f32[3072]{0:T(1024)S(1)}, f32[3072]{0:T(1024)S(1)}) all-reduce(f32[4,512]{1,0:T(4,128)S(1)} %get-tuple-element.36, f32[3072]{0:T(1024)S(1)} %get-tuple-element.37, f32[3072]{0:T(1024)S(1)} %get-tuple-element.38), channel_id=1, replica_groups=mesh['sp_0'=8,'sp_1'=8,'dp_0'=4,'dp_1'=2] {'sp_1'}, use_global_device_ids=true, to_apply=%region_9.10 | all-reduce | flops 8192 | bytes 65536 | tf_op jit(solution)/shard_map/psum | solution.py:50
  257.7 12.1 %all-reduce.2 = (f32[4,512]{1,0:T(4,128)S(1)}, f32[3072]{0:T(1024)S(1)}, f32[3072]{0:T(1024)S(1)}) all-reduce(f32[4,512]{1,0:T(4,128)S(1)} %get-tuple-element.33, f32[3072]{0:T(1024)S(1)} %get-tuple-element.34, f32[3072]{0:T(1024)S(1)} %get-tuple-element.35), channel_id=1, replica_groups=mesh['sp_0'=8,'sp_1'=8,'dp_0'=4,'dp_1'=2] {'dp_0'}, use_global_device_ids=true, to_apply=%region_10.11 | all-reduce | flops 8192 | bytes 65536 | tf_op jit(solution)/shard_map/psum | solution.py:50
  269.8 21.1 %all-reduce.3 = (f32[4,512]{1,0:T(4,128)}, f32[3072]{0:T(1024)}, f32[3072]{0:T(1024)}) all-reduce(f32[4,512]{1,0:T(4,128)S(1)} %get-tuple-element.39, f32[3072]{0:T(1024)S(1)} %get-tuple-element.40, f32[3072]{0:T(1024)S(1)} %get-tuple-element.41), channel_id=1, replica_groups=mesh['sp_0'=8,'sp_1'=8,'dp_0'=4,'dp_1'=2] {'dp_1'}, use_global_device_ids=true, to_apply=%region_11.12 | all-reduce | flops 8192 | bytes 65536 | tf_op jit(solution)/shard_map/psum | solution.py:50
  292.3 1.9 copy.67
  (55 shorter events, 22.5 us)
Async XLA Ops:
  0.6 1.0 copy-start
  1.8 11.1 %copy-start.2 = (bf16[1,128,3072]{2,1,0:T(8,128)(2,1)S(1)}, bf16[1,128,3072]{2,1,0:T(8,128)(2,1)}, u32[]{:S(2)}) copy-start(bf16[1,128,3072]{2,1,0:T(8,128)(2,1)} %param.9) | copy-start | bytes 2359300
  2.6 19.6 %all-to-all-start.1 = ((bf16[8,64,512]{2,1,0:T(8,128)(2,1)}), bf16[8,64,512]{2,1,0:T(8,128)(2,1)S(1)}, u32[]{:S(2)}, u32[]{:S(2)}) async-start(bf16[8,64,512]{2,1,0:T(8,128)(2,1)} %broadcast_in_dim.10), calls=%async_computation.1 | async-start | bytes 1048576 | tf_op jit(solution)/shard_map/all_to_all | solution.py:24
  12.8 1.1 copy-start.3
  22.2 33.3 %all-to-all-start.3 = ((bf16[64,48,128]{2,1,0:T(8,128)(2,1)}), bf16[64,48,128]{2,1,0:T(8,128)(2,1)S(1)}, u32[]{:S(2)}, u32[]{:S(2)}) async-start(bf16[64,48,128]{2,1,0:T(8,128)(2,1)} %bitcast.16), calls=%async_computation.3 | async-start | bytes 1572864 | tf_op jit(solution)/shard_map/all_to_all | solution.py:73
  56.2 2.8 copy-start.4
  61.9 28.9 %all-to-all-start.4 = ((bf16[48,64,128]{2,0,1:T(8,128)(2,1)}), bf16[48,64,128]{2,0,1:T(8,128)(2,1)S(1)}, u32[]{:S(2)}, u32[]{:S(2)}) async-start(bf16[48,64,128]{2,0,1:T(8,128)(2,1)} %copy.58), calls=%async_computation.4 | async-start | bytes 1572864 | tf_op jit(solution)/shard_map/all_to_all | solution.py:91
  71.4 19.4 %copy-start.6 = (f32[3072]{0:T(1024)S(1)}, f32[3072]{0:T(1024)}, u32[]{:S(2)}) copy-start(f32[3072]{0:T(1024)} %param.10) | copy-start | bytes 36868
  72.3 19.5 %copy-start.7 = (f32[3072]{0:T(1024)S(1)}, f32[3072]{0:T(1024)}, u32[]{:S(2)}) copy-start(f32[3072]{0:T(1024)} %param.11) | copy-start | bytes 36868
  126.1 18.3 %all-to-all-start.5 = ((bf16[8,64,512]{2,1,0:T(8,128)(2,1)}), bf16[8,64,512]{2,1,0:T(8,128)(2,1)S(1)}, u32[]{:S(2)}, u32[]{:S(2)}) async-start(bf16[8,64,512]{2,1,0:T(8,128)(2,1)} %bitcast.102), calls=%async_computation.5 | async-start | bytes 1048576 | tf_op jit(solution)/shard_map/all_to_all | solution.py:38
  144.5 7.9 %copy-start.5 = (bf16[48,16,512]{2,1,0:T(8,128)(2,1)S(1)}, bf16[48,16,512]{2,1,0:T(8,128)(2,1)}, u32[]{:S(2)}) copy-start(bf16[48,16,512]{2,1,0:T(8,128)(2,1)} %reshape.195) | copy-start | bytes 2359300
  145.5 22.7 %all-to-all-start.6 = ((f32[64,1,4,512]{3,2,1,0:T(4,128)}), f32[64,1,4,512]{3,2,1,0:T(4,128)}, u32[]{:S(2)}, u32[]{:S(2)}) async-start(f32[64,1,4,512]{3,2,1,0:T(4,128)} %broadcast_multiply_fusion), calls=%async_computation.6 | async-start | bytes 1048576 | tf_op jit(solution)/shard_map/all_to_all | solution.py:44
  168.2 28.0 %all-to-all-start.2 = ((bf16[48,64,128]{2,0,1:T(8,128)(2,1)}), bf16[48,64,128]{2,0,1:T(8,128)(2,1)S(1)}, u32[]{:S(2)}, u32[]{:S(2)}) async-start(bf16[48,64,128]{2,0,1:T(8,128)(2,1)} %copy.55), calls=%async_computation.2 | async-start | bytes 1572864 | tf_op jit(solution)/shard_map/all_to_all | solution.py:88
  197.0 9.1 %copy-start.1 = (bf16[128,3072]{0,1:T(8,128)(2,1)S(1)}, bf16[128,3072]{0,1:T(8,128)(2,1)}, u32[]{:S(2)}) copy-start(bf16[128,3072]{0,1:T(8,128)(2,1)} %get-tuple-element.45) | copy-start | bytes 2359300
  197.0 95.3 %all-to-all-start.7 = ((f32[64,1,4,512]{3,2,1,0:T(4,128)}), f32[64,1,4,512]{3,2,1,0:T(4,128)}, u32[]{:S(2)}, u32[]{:S(2)}) async-start(f32[64,1,4,512]{3,2,1,0:T(4,128)} %broadcast_in_dim.14), calls=%async_computation.7 | async-start | bytes 1048576 | tf_op jit(solution)/shard_map/all_to_all | solution.py:24
where the time goes:
time: 295 us; the launch traced here: 294 us
  blocking collectives  111 us (38%)
  waiting for transfers between devices  85 us (29%)
  starting transfers between devices  60.7 us (21%)
  local copies, waits for them, and re-layouts  18.9 us (6%)
  other arithmetic  9.45 us (3%)
  matrix products  8.07 us (3%)
    psum x4, blocking collectives, by_axis(): x = lax.psum(x, axis)  83.6 us
    all_to_all x1, blocking collectives, by_groups(): lax.all_to_all(normed.T, SP, split_axis=0, concat_axis=1, tiled=True)  27.6 us
    all_to_all x1, waiting for transfers between devices, by_groups(): lax.all_to_all(mix_grad.T, SP, split_axis=0, concat_axis=1, tiled=True)  20.4 us
    all_to_all x1, waiting for transfers between devices, by_groups(): lax.all_to_all(mixed_b.reshape(channels, seq_len), SP, split_axis=1, conc...  19.6 us
    all_to_all x2, starting transfers between devices, sent_to_all(): return lax.all_to_all(copies, axis, split_axis=0, concat_axis=0, tiled=True)  18.7 us
    all_to_all x1, waiting for transfers between devices, by_groups(): lax.all_to_all(back_b.reshape(channels, seq_len), SP, split_axis=1, conca...  18.5 us
    all_to_all x1, starting transfers between devices, by_groups(): lax.all_to_all(mix_grad.T, SP, split_axis=0, concat_axis=1, tiled=True)  11.8 us
    all_to_all x1, waiting for transfers between devices, sum_at_owner_2(): pieces = lax.all_to_all(cut_along(x, dim, devices), axis, 0, 0, tiled=True)  10.3 us
  transfers between devices with their start and end apart: 7, of which 6 were waited for; matrix products, arithmetic and copies ran while one was open for 5% of the time, Pallas kernels for 0%

commit v1 on v0

v1 whole, which is shorter than its diff:
```python
import jax
import jax.numpy as jnp
from jax import lax
from jax.experimental import pallas as pl
from jax.experimental.pallas import tpu as pltpu
from jax.sharding import Mesh
from jax.sharding import PartitionSpec as P

AXES = ("z", "y", "x", "core")
DP = ("x", "core")
SP = ("z", "y")
MESH = pl.DeviceIdType.MESH
F32 = jnp.float32
BF16 = jnp.bfloat16
EPS = 1e-05

GROUPS = 4
ROWS = 128
WIDTH = 3072
CHUNKS = 8
CW = WIDTH // CHUNKS

TILES = {
    (0, 0): [(0, g) for g in range(4)],
    (1, 1): [(0, g) for g in range(4)] + [(1, g) for g in range(4)],
    (1, 2): [(0, 2), (0, 3), (1, 2), (1, 3)],
    (1, 3): [(0, 2), (0, 3), (1, 2), (1, 3)],
    (2, 2): [(2, g) for g in range(4)] + [(0, 0), (0, 1), (1, 0), (1, 1)],
    (2, 3): [(2, g) for g in range(4)] + [(0, 0), (0, 1), (1, 0), (1, 1)],
    (3, 3): [(3, g) for g in range(4)],
}
PIECES = {
    (0, 0): [(0, 4, 0, 128)],
    (1, 1): [(0, 4, 0, 256)],
    (1, 2): [(2, 4, 0, 256)],
    (1, 3): [(2, 4, 0, 256)],
    (2, 2): [(0, 4, 256, 384), (0, 2, 0, 256)],
    (2, 3): [(0, 4, 256, 384), (0, 2, 0, 256)],
    (3, 3): [(0, 4, 384, 512)],
}


def remote(src, dst, send, recv, device):
    return pltpu.make_async_remote_copy(
        src_ref=src, dst_ref=dst, send_sem=send, recv_sem=recv, device_id=device, device_id_type=MESH
    )


def dot(a, b):
    return jnp.dot(a, b, preferred_element_type=F32)


def dot_t(a, b):
    return lax.dot_general(a, b, (((1,), (1,)), ((), ())), preferred_element_type=F32)


def loop(lo, hi, body):
    lax.fori_loop(lo, hi, lambda i, _: (body(i), None)[1], None)


def kernel(
    gated, values, upstream, gain, shift, wt, bias,
    out_u, out_v, out_mix, out_vec,
    XC, YC, UN, INV, RES, YP, PS1, PS2, PSQ, PR, PQ, ACC,
    WBUF, WX, WXT, BIASC, GX, GS, GR, GZ, ZR, YS, YR, ZS, ZG,
    VS, VA, VT, VB, VU, VC, VW, VD,
    w_s, w_r, m_s, m_r, r1_s, r1_r, r2_s, r2_r, r3_s, r3_r, r4_s, r4_r,
    v1_s, v1_r, v2_s, v2_r, v3_s, v3_r, v4_s, v4_r,
):
    z, y = lax.axis_index("z"), lax.axis_index("y")
    x, core = lax.axis_index("x"), lax.axis_index("core")
    d = x * 2 + core
    half = y // 4
    j = y % 4
    up = j // 2
    inner = (j == 1) | (j == 2)
    lower = up == 0
    upper = up == 1
    base = half * 4
    own_outer = (z, base + 3 * up, x, core)
    own_inner = (z, base + 1 + up, x, core)
    opp_inner = (z, base + 2 - up, x, core)
    opp_outer = (z, base + 3 - 3 * up, x, core)
    kx, ky = up, 1 - up

    def dp_peer(o):
        e = (d + o) % 8
        return e, (z, y, e // 2, e % 2)

    def z_peer(o):
        e = (z + o) % 8
        return e, (e, y, x, core)

    def y_peer(o):
        e = (y + o) % 8
        return e, (z, e, x, core)

    def phys(q):
        return (q + 4 * up) % 8

    barrier = pltpu.get_barrier_semaphore()

    def greet(o):
        for peer in (dp_peer, z_peer, y_peer):
            pl.semaphore_signal(barrier, inc=1, device_id=peer(o)[1], device_id_type=MESH)

    loop(1, 8, greet)

    def norm(i):
        r = pl.multiple_of(i * 16, 16)
        v = values[0, pl.ds(r, 16), :].astype(F32)
        d0 = v - jnp.sum(v, axis=1, keepdims=True) * (1.0 / WIDTH)
        inv = lax.rsqrt(jnp.sum(d0 * d0, axis=1, keepdims=True) * (1.0 / WIDTH) + EPS)
        INV[pl.ds(r, 16), :] = jnp.broadcast_to(inv, (16, 128))
        u = d0 * inv
        n = (u * gain[...] + shift[...]).astype(BF16)
        m = (upstream[0, pl.ds(r, 16), :].astype(F32) * gated[0, pl.ds(r, 16), :].astype(F32)).astype(BF16)
        for c in range(CHUNKS):
            UN[c, pl.ds(r, 16), :] = u[:, c * CW : (c + 1) * CW]

        def put(a, b):
            for c in range(CHUNKS):
                XC[c, pl.ds(r + ROWS, 16), :] = a[:, c * CW : (c + 1) * CW]
                YC[c, pl.ds(r, 16), :] = b[:, c * CW : (c + 1) * CW]

        @pl.when(lower)
        def _():
            put(n, m)

        @pl.when(upper)
        def _():
            put(m, n)

    loop(0, 8, norm)

    pl.semaphore_wait(barrier, 21)

    for (jj, t), pieces in PIECES.items():

        @pl.when((j == jj) & (x == t))
        def _(t=t, pieces=pieces):
            def send(o):
                e, peer = dp_peer(o)
                for i, (g0, g1, c0, c1) in enumerate(pieces):
                    remote(
                        wt.at[g0:g1, :, c0:c1],
                        WBUF.at[t, g0:g1, pl.ds(core * 64, 64), c0:c1],
                        w_s.at[e, i],
                        w_r.at[d, i],
                        peer,
                    ).start()

            loop(1, 8, send)

    def x_near(c, to):
        return remote(XC.at[c, pl.ds(ROWS, ROWS), :], XC.at[c, pl.ds(0, ROWS), :], m_s.at[0, c], m_r.at[0, c], to)

    def x_far(c):
        return remote(
            XC.at[c, pl.ds(ROWS, ROWS), :], YC.at[c, pl.ds(2 * ROWS, ROWS), :], m_s.at[1, c], m_r.at[2, c], opp_inner
        )

    def x_opp(c):
        return remote(
            XC.at[c, pl.ds(ROWS, ROWS), :], YC.at[c, pl.ds(ROWS, ROWS), :], m_s.at[0, c], m_r.at[1, c], opp_inner
        )

    def p_inner(c):
        return remote(PS1.at[c], PR.at[c], m_s.at[1, c], m_r.at[3, c], opp_inner)

    def p_outer(c):
        return remote(PS2.at[c], PR.at[c], m_s.at[2, c], m_r.at[3, c], opp_outer)

    def q_outer(c):
        return remote(PSQ.at[c], PQ.at[c], m_s.at[3, c], m_r.at[4, c], own_outer)

    @pl.when(inner)
    def _():
        loop(0, 4, lambda q: x_opp(phys(q)).start())

    @pl.when(jnp.logical_not(inner))
    def _():
        def send(q):
            x_near(phys(q + 4), own_inner).start()
            x_far(phys(q)).start()

        loop(0, 4, send)
        loop(0, 4, lambda q: x_near(phys(q), own_inner).start())

    VS[...] = jnp.zeros_like(VS)
    GX[...] = jnp.zeros_like(GX)
    ones = jnp.ones((8, CW), BF16)
    for g in range(GROUPS):
        rows = jnp.broadcast_to(bias[pl.ds(g, 1), pl.ds(pl.multiple_of(j * 128, 128), 128)], (128, 128))
        BIASC[g] = rows.T

    def sum_bias(source, row0):
        for g in range(GROUPS):
            s = dot_t(ones, source[2 * g, pl.ds(row0, ROWS), :]) + dot_t(ones, source[2 * g + 1, pl.ds(row0, ROWS), :])
            VS[6 + g // 2, pl.ds((g % 2) * 4 + j, 1), :] = s[0:1]

    @pl.when(lower)
    def _():
        sum_bias(YC, 0)

    @pl.when(upper)
    def _():
        sum_bias(XC, ROWS)

    WBUF[x, :, pl.ds(pl.multiple_of(core * 64, 64), 64), :] = wt[...]
    for (jj, t), pieces in PIECES.items():
        for cc in range(2):

            @pl.when((j == jj) & (d != 2 * t + cc))
            def _(t=t, cc=cc, pieces=pieces):
                for i, (g0, g1, c0, c1) in enumerate(pieces):
                    there = WBUF.at[t, g0:g1, cc * 64 : cc * 64 + 64, c0:c1]
                    remote(there, there, w_s.at[0, i], w_r.at[2 * t + cc, i], own_inner).wait_recv()

    seg_t = lax.broadcasted_iota(jnp.int32, (128, 128), 0) // 64
    seg_s = lax.broadcasted_iota(jnp.int32, (128, 128), 1) // 64
    allowed = seg_t >= seg_s

    def tile(t, s, g):
        w = WBUF[t, g, :, s * 128 : (s + 1) * 128]
        return jnp.where(allowed, w, jnp.zeros_like(w)) if t == s else w

    def place(g, dst, src, a, b):
        WX[g, dst * 128 : (dst + 1) * 128, src * 128 : (src + 1) * 128] = a
        WXT[g, src * 128 : (src + 1) * 128, dst * 128 : (dst + 1) * 128] = b

    @pl.when(j == 0)
    def _():
        for g in range(GROUPS):
            w = tile(0, 0, g)
            place(g, 0, 0, w, w.T)

    @pl.when(j == 3)
    def _():
        for g in range(GROUPS):
            w = tile(3, 3, g)
            place(g, 0, 0, w.T, w)

    @pl.when(j == 1)
    def _():
        for g in range(GROUPS):
            for t in (1, 2, 3) if g >= 2 else (1,):
                for s in (0, 1):
                    w = tile(t, s, g)
                    place(g, t - 1, s, w, w.T)

    @pl.when(j == 2)
    def _():
        for g in range(GROUPS):
            for s in (0, 1, 2) if g < 2 else (2,):
                for t in (2, 3):
                    w = tile(t, s, g)
                    place(g, 2 - s, 3 - t, w.T, w)

    def bias_of(g, on):
        b = jnp.where(on, BIASC[g], 0.0)
        return jnp.concatenate([b] * (CW // 128), axis=1)

    def put_x(c, g, value):
        RES[kx, c] = (value + bias_of(g, lower)).astype(BF16)

    def put_y(c, g, value):
        RES[ky, c] = (value + bias_of(g, upper)).astype(BF16)

    @pl.when(inner)
    def _():
        def early(q):
            c = phys(q)
            s = dot(WXT[c // 2, :, 0:ROWS], YC[c, 0:ROWS, :])
            PSQ[c] = s[0:ROWS].astype(BF16)
            YP[c] = s[ROWS:]
            q_outer(c).start()

        loop(0, 4, early)

        def second(i):
            c = phys(i + 4)
            g = c // 2
            x_near(c, own_outer).wait_recv()
            r = dot(WX[g], XC[c])
            PS1[c] = r[ROWS : 2 * ROWS].astype(BF16)
            PS2[c] = r[2 * ROWS :].astype(BF16)
            put_x(c, g, r[0:ROWS])
            p_outer(c).start()
            p_inner(c).start()
            x_opp(c).wait_recv()
            x_far(c).wait_recv()
            s = dot(WXT[g], YC[c])
            PSQ[c] = s[0:ROWS].astype(BF16)
            put_y(c, g, s[ROWS:])
            q_outer(c).start()
            GX[g] += dot_t(YC[c], XC[c])

        loop(0, 4, second)

        def first(q):
            c = phys(q)
            g = c // 2
            x_near(c, own_outer).wait_recv()
            put_x(c, g, dot(WX[g, 0:ROWS, :], XC[c]))
            GX[g, 0:ROWS, :] += dot_t(YC[c, 0:ROWS, :], XC[c])

        loop(0, 4, first)

    @pl.when(jnp.logical_not(inner))
    def _():
        def local(c):
            g = c // 2
            own_x = XC[c, pl.ds(ROWS, ROWS), :]
            own_y = YC[c, pl.ds(0, ROWS), :]
            put_x(c, g, dot(WX[g, 0:ROWS, 0:ROWS], own_x))
            YP[c] = dot(WXT[g, 0:ROWS, 0:ROWS], own_y)
            GX[g, 0:ROWS, 0:ROWS] += dot_t(own_y, own_x)

        loop(0, 8, local)

    def stage(t, index, value):
        value = value.astype(BF16)
        GS[t, 0, index] = value[0:64]
        GS[t, 1, index] = value[64:128]

    for (jj, t), tiles in TILES.items():

        @pl.when(j == jj)
        def _(jj=jj, t=t, tiles=tiles):
            for index, (s, g) in enumerate(tiles):
                if jj == 0:
                    value = GX[g, 0:128, 0:128]
                elif jj == 3:
                    value = GX[g, 0:128, 0:128].T
                elif jj == 1:
                    value = GX[g, (t - 1) * 128 : t * 128, s * 128 : (s + 1) * 128]
                else:
                    value = GX[g, (2 - s) * 128 : (3 - s) * 128, (3 - t) * 128 : (4 - t) * 128].T
                stage(t, index, value)
            n = len(tiles)
            for h in range(2):
                e = 2 * t + h

                @pl.when(d != e)
                def _():
                    remote(
                        GS.at[t, h, 0:n], GR.at[d, 0:n], r1_s.at[e], r1_r.at[d], (z, y, t, h)
                    ).start()

                @pl.when(d == e)
                def _():
                    GR[e, 0:n] = GS[t, h, 0:n]

    @pl.when(inner)
    def _():
        def late(q):
            c = phys(q)
            p_inner(c).wait_recv()
            put_y(c, c // 2, YP[c] + PR[c].astype(F32))

        loop(0, 4, late)

    @pl.when(jnp.logical_not(inner))
    def _():
        def late(q):
            c = phys(q)
            p_outer(c).wait_recv()
            q_outer(c).wait_recv()
            put_y(c, c // 2, YP[c] + PR[c].astype(F32) + PQ[c].astype(F32))

        loop(0, 4, late)

        def later(q):
            c = phys(q)
            q_outer(c).wait_recv()
            put_y(c, c // 2, YP[c] + PQ[c].astype(F32))

        loop(4, 8, later)

    def each_owned(body):
        for (jj, t), tiles in TILES.items():

            @pl.when((j == jj) & (x == t))
            def _(jj=jj, t=t, tiles=tiles):
                body(jj, t, tiles)

    def sum_dp(jj, t, tiles):
        n = len(tiles)

        def wait(o):
            e, peer = dp_peer(o)
            remote(GR.at[e, 0:n], GR.at[e, 0:n], r1_s.at[0], r1_r.at[e], peer).wait_recv()

        loop(1, 8, wait)

        def add(i):
            total = GR[0, i].astype(F32)
            for e in range(1, 8):
                total = total + GR[e, i].astype(F32)
            total = total.astype(BF16)
            for rs in range(4):
                GZ[rs, i] = total[rs * 16 : (rs + 1) * 16]

        loop(0, n, add)
        m = n // 2

        def send(o):
            e, peer = z_peer(o)
            remote(
                GZ.at[e % 4, pl.ds((e // 4) * m, m)], ZR.at[z, 0:m], r2_s.at[e], r2_r.at[z], peer
            ).start()

        loop(1, 8, send)
        ZR[z, 0:m] = GZ[z % 4, pl.ds((z // 4) * m, m)]

    each_owned(sum_dp)

    ACC[...] = jnp.zeros_like(ACC)

    def sums(c):
        back = RES[1, c].astype(F32)
        u = UN[c]
        g = gain[:, pl.ds(pl.multiple_of(c * CW, 128), CW)]
        bu = back * u
        a, b = back * g, bu * g
        ACC[0] += a[:, 0:128] + a[:, 128:256] + a[:, 256:384]
        ACC[1] += b[:, 0:128] + b[:, 128:256] + b[:, 256:384]
        gt = jnp.sum(bu, axis=0, keepdims=True)
        st = jnp.sum(back, axis=0, keepdims=True)
        for i in range(3):
            row = c * 3 + i
            VS[row // 8, pl.ds(row % 8, 1), :] = gt[:, i * 128 : (i + 1) * 128]
            VS[row // 8 + 3, pl.ds(row % 8, 1), :] = st[:, i * 128 : (i + 1) * 128]

    loop(0, CHUNKS, sums)

    def vec_send(source, land, me, send, recv, peer):
        def one(o):
            e, to = peer(o)
            remote(source(e), land.at[me], send.at[e], recv.at[me], to).start()

        loop(1, 8, one)

    def vec_wait(land, send, recv, peer):
        def one(o):
            e, to = peer(o)
            remote(land.at[e], land.at[e], send.at[e], recv.at[e], to).wait_recv()

        loop(1, 8, one)

    def vec_sum(land):
        total = land[0]
        for e in range(1, 8):
            total = total + land[e]
        return total

    vec_send(lambda e: VS.at[e], VA, d, v1_s, v1_r, dp_peer)
    VA[d] = VS[d]

    def sum_z(jj, t, tiles):
        m = len(tiles) // 2

        def wait(o):
            e, peer = z_peer(o)
            remote(ZR.at[e, 0:m], ZR.at[e, 0:m], r2_s.at[0], r2_r.at[e], peer).wait_recv()

        loop(1, 8, wait)
        total = ZR[0, 0:m].astype(F32)
        for e in range(1, 8):
            total = total + ZR[e, 0:m].astype(F32)
        YS[0:m] = total.astype(BF16)

        def send(o):
            e, peer = y_peer(o)
            remote(YS.at[0:m], YR.at[y, 0:m], r3_s.at[e], r3_r.at[y], peer).start()

        loop(1, 8, send)
        YR[y, 0:m] = YS[0:m]

    each_owned(sum_z)

    vec_wait(VA, v1_s, v1_r, dp_peer)
    VT[...] = vec_sum(VA)
    vec_send(lambda e: VT, VB, z, v2_s, v2_r, z_peer)
    VB[z] = VT[...]

    mean_a = jnp.sum(ACC[0], axis=1, keepdims=True) * (1.0 / WIDTH)
    mean_b = jnp.sum(ACC[1], axis=1, keepdims=True) * (1.0 / WIDTH)
    ACC[0] = jnp.broadcast_to(mean_a, (ROWS, 128))
    ACC[1] = jnp.broadcast_to(mean_b, (ROWS, 128))

    def wide(v):
        return jnp.concatenate([v] * (CW // 128), axis=1)

    def outputs(c):
        cols = pl.ds(pl.multiple_of(c * CW, 128), CW)
        scaled = RES[1, c].astype(F32) * gain[:, cols]
        out_v[0, :, cols] = (wide(INV[...]) * (scaled - wide(ACC[0]) - UN[c] * wide(ACC[1]))).astype(BF16)
        out_u[0, :, cols] = (upstream[0, :, cols].astype(F32) * RES[0, c].astype(F32)).astype(BF16)

    loop(0, CHUNKS, outputs)

    vec_wait(VB, v2_s, v2_r, z_peer)
    VU[...] = vec_sum(VB)
    vec_send(lambda e: VU, VC, y, v3_s, v3_r, y_peer)
    VC[y] = VU[...]

    for t in range(4):
        places = [(jj, tiles) for (jj, tt), tiles in TILES.items() if tt == t]
        total_tiles = sum(len(tiles) // 2 for _, tiles in places)

        @pl.when(x == t)
        def _(t=t, places=places, total_tiles=total_tiles):
            off = 0
            for jj, tiles in places:
                m = len(tiles) // 2
                for yy in (jj, jj + 4):

                    @pl.when(y != yy)
                    def _():
                        there = YR.at[yy, 0:m]
                        remote(there, there, r3_s.at[0], r3_r.at[yy], own_inner).wait_recv()

                for i in range(m):
                    ZS[off + i] = (YR[jj, i].astype(F32) + YR[jj + 4, i].astype(F32)).astype(BF16)
                off += m

            def send(o):
                e, peer = z_peer(o)
                remote(ZS.at[0:total_tiles], ZG.at[z, 0:total_tiles], r4_s.at[e], r4_r.at[z], peer).start()

            loop(1, 8, send)
            ZG[z, 0:total_tiles] = ZS[0:total_tiles]

    vec_wait(VC, v3_s, v3_r, y_peer)
    VW[...] = vec_sum(VC)
    vec_send(lambda e: VW, VD, d, v4_s, v4_r, dp_peer)
    VD[d] = VW[...]

    out_mix[...] = jnp.zeros_like(out_mix)
    keep = lax.broadcasted_iota(jnp.int32, (16, 128), 1) // 64 <= core
    for t in range(4):
        places = [(jj, tiles) for (jj, tt), tiles in TILES.items() if tt == t]
        total_tiles = sum(len(tiles) // 2 for _, tiles in places)

        @pl.when(x == t)
        def _(t=t, places=places, total_tiles=total_tiles):
            def wait(o):
                e, peer = z_peer(o)
                there = ZG.at[e, 0:total_tiles]
                remote(there, there, r4_s.at[0], r4_r.at[e], peer).wait_recv()

            loop(1, 8, wait)
            for k in range(8):
                rows = slice(16 * (k % 4), 16 * (k % 4) + 16)
                off = 0
                for jj, tiles in places:
                    m = len(tiles) // 2
                    for i in range(m):
                        s, g = tiles[(k // 4) * m + i]
                        value = ZG[k, off + i].astype(F32)
                        if s == t:
                            value = jnp.where(keep, value, 0.0)
                        out_mix[g, rows, s * 128 : (s + 1) * 128] = value
                    off += m

    vec_wait(VD, v4_s, v4_r, dp_peer)
    out_vec[...] = VD[...]

    for (jj, t), pieces in PIECES.items():

        @pl.when((j == jj) & (x == t))
        def _(t=t, pieces=pieces):
            def wait(o):
                e, peer = dp_peer(o)
                for i, (g0, g1, c0, c1) in enumerate(pieces):
                    remote(
                        wt.at[g0:g1, :, c0:c1],
                        WBUF.at[t, g0:g1, pl.ds(core * 64, 64), c0:c1],
                        w_s.at[e, i],
                        w_r.at[d, i],
                        peer,
                    ).wait_send()

            loop(1, 8, wait)

    @pl.when(inner)
    def _():
        def wait(q):
            x_opp(phys(q)).wait_send()
            p_outer(phys(q + 4)).wait_send()
            p_inner(phys(q + 4)).wait_send()

        loop(0, 4, wait)
        loop(0, 8, lambda q: q_outer(phys(q)).wait_send())

    @pl.when(jnp.logical_not(inner))
    def _():
        loop(0, 4, lambda q: x_far(phys(q)).wait_send())
        loop(0, 8, lambda q: x_near(phys(q), own_inner).wait_send())

    for (jj, t), tiles in TILES.items():
        n = len(tiles)
        for h in range(2):

            @pl.when((j == jj) & (d != 2 * t + h))
            def _(t=t, h=h, n=n):
                remote(
                    GS.at[t, h, 0:n], GR.at[d, 0:n], r1_s.at[2 * t + h], r1_r.at[d], (z, y, t, h)
                ).wait_send()

    def sent(jj, t, tiles):
        m = len(tiles) // 2

        def one(o):
            e, peer = z_peer(o)
            remote(GZ.at[0, 0:m], ZR.at[z, 0:m], r2_s.at[e], r2_r.at[z], peer).wait_send()
            e, peer = y_peer(o)
            remote(YS.at[0:m], YR.at[y, 0:m], r3_s.at[e], r3_r.at[y], peer).wait_send()

        loop(1, 8, one)

    each_owned(sent)
    for t in range(4):
        total_tiles = sum(len(tiles) // 2 for (_, tt), tiles in TILES.items() if tt == t)

        @pl.when(x == t)
        def _(total_tiles=total_tiles):
            def one(o):
                e, peer = z_peer(o)
                remote(ZS.at[0:total_tiles], ZG.at[z, 0:total_tiles], r4_s.at[e], r4_r.at[z], peer).wait_send()

            loop(1, 8, one)

    def vec_sent(o):
        for source, land, me, send, recv, peer in (
            (VS.at[0], VA, d, v1_s, v1_r, dp_peer),
            (VT, VB, z, v2_s, v2_r, z_peer),
            (VU, VC, y, v3_s, v3_r, y_peer),
            (VW, VD, d, v4_s, v4_r, dp_peer),
        ):
            e, to = peer(o)
            remote(source, land.at[me], send.at[e], recv.at[me], to).wait_send()

    loop(1, 8, vec_sent)


def per_device(gated, values_in, upstream, gain, shift, mix_w, mix_bias):
    vmem = pl.BlockSpec(memory_space=pltpu.VMEM)
    chunks = (CHUNKS, ROWS, CW)
    dma = pltpu.SemaphoreType.DMA
    out_u, out_v, out_mix, out_vec = pl.pallas_call(
        kernel,
        out_shape=(
            jax.ShapeDtypeStruct((1, ROWS, WIDTH), BF16),
            jax.ShapeDtypeStruct((1, ROWS, WIDTH), BF16),
            jax.ShapeDtypeStruct((GROUPS, 64, 512), F32),
            jax.ShapeDtypeStruct((8, 8, 128), F32),
        ),
        in_specs=[vmem] * 7,
        out_specs=[vmem] * 4,
        scratch_shapes=[
            pltpu.VMEM((CHUNKS, 2 * ROWS, CW), BF16),
            pltpu.VMEM((CHUNKS, 3 * ROWS, CW), BF16),
            pltpu.VMEM(chunks, F32),
            pltpu.VMEM((ROWS, 128), F32),
            pltpu.VMEM((2, *chunks), BF16),
            pltpu.VMEM(chunks, F32),
            pltpu.VMEM(chunks, BF16),
            pltpu.VMEM(chunks, BF16),
            pltpu.VMEM(chunks, BF16),
            pltpu.VMEM(chunks, BF16),
            pltpu.VMEM(chunks, BF16),
            pltpu.VMEM((2, ROWS, 128), F32),
            pltpu.VMEM((4, GROUPS, 128, 512), BF16),
            pltpu.VMEM((GROUPS, 384, 256), BF16),
            pltpu.VMEM((GROUPS, 256, 384), BF16),
            pltpu.VMEM((GROUPS, 128, 128), F32),
            pltpu.VMEM((GROUPS, 384, 256), F32),
            pltpu.VMEM((4, 2, 8, 64, 128), BF16),
            pltpu.VMEM((8, 8, 64, 128), BF16),
            pltpu.VMEM((4, 8, 16, 128), BF16),
            pltpu.VMEM((8, 4, 16, 128), BF16),
            pltpu.VMEM((4, 16, 128), BF16),
            pltpu.VMEM((8, 4, 16, 128), BF16),
            pltpu.VMEM((8, 16, 128), BF16),
            pltpu.VMEM((8, 8, 16, 128), BF16),
            pltpu.VMEM((8, 8, 128), F32),
            pltpu.VMEM((8, 8, 128), F32),
            pltpu.VMEM((8, 128), F32),
            pltpu.VMEM((8, 8, 128), F32),
            pltpu.VMEM((8, 128), F32),
            pltpu.VMEM((8, 8, 128), F32),
            pltpu.VMEM((8, 128), F32),
            pltpu.VMEM((8, 8, 128), F32),
            dma((8, 2)), dma((8, 2)), dma((4, 8)), dma((5, 8)),
            *[dma((8,)) for _ in range(16)],
        ],
        compiler_params=pltpu.CompilerParams(
            collective_id=0, has_side_effects=True, vmem_limit_bytes=48 * 1024 * 1024
        ),
        name="span",
    )(
        gated,
        values_in,
        upstream,
        gain.reshape(1, WIDTH),
        shift.reshape(1, WIDTH),
        mix_w.transpose(1, 0, 2),
        mix_bias,
    )
    vec = out_vec.reshape(64 * 128)
    return (
        out_u,
        out_v,
        out_mix.transpose(1, 0, 2),
        vec[2 * WIDTH :].reshape(GROUPS, 512),
        vec[:WIDTH],
        vec[WIDTH : 2 * WIDTH],
    )


def solution(mesh):
    torus = Mesh(mesh.devices.reshape(8, 8, 4, 2), AXES)
    return jax.shard_map(
        per_device,
        mesh=torus,
        in_specs=(
            P(DP, SP, None),
            P(DP, SP, None),
            P(DP, SP, None),
            P(),
            P(),
            P(DP, None, None),
            P(),
        ),
        out_specs=(P(DP, SP, None), P(DP, SP, None), P(DP, None, None), P(), P(), P()),
        check_vma=False,
    )
```

time: 295 us -> 82.9 us (0.28)
  blocking collectives: 111 us -> 0 us
  waiting for transfers between devices: 85 us -> 0 us
  Pallas kernels: 0 us -> 73.4 us
  starting transfers between devices: 60.7 us -> 0 us
  local copies, waits for them, and re-layouts: 18.9 us -> 8.53 us
  other arithmetic: 9.45 us -> 0 us
  matrix products: 8.07 us -> 0 us
    all_to_all x7 -> x0, waiting for transfers between devices: 85 us -> none  [the longest x1 20.4 us: by_groups(): lax.all_to_all(mix_grad.T, SP, split_axis=0, concat_axis=1, tiled=True)]
    psum x4 -> x0, blocking collectives: 83.6 us -> none  [by_axis(): x = lax.psum(x, axis)]
    pallas_call x0 -> x1, Pallas kernels: none -> 73.4 us  [per_device(): pl.pallas_call(kernel, out_shape=(jax.ShapeDtypeStruct((1, ROWS, WIDTH),...]
    all_to_all x7 -> x0, starting transfers between devices: 60.7 us -> none  [the longest x2 18.7 us: sent_to_all(): return lax.all_to_all(copies, axis, split_axis=0, concat_axis=0, tiled=True)]
    all_to_all x1 -> x0, blocking collectives: 27.6 us -> none  [by_groups(): lax.all_to_all(normed.T, SP, split_axis=0, concat_axis=1, tiled=True)]
    dot_general x3 -> x0, matrix products: 8.07 us -> none  [the longest x1 2.77 us: by_groups(): jnp.einsum('ts,cnt->cns', weights, grad_blocks, preferred_element_type=jn...]
    all_to_all x6 -> x0, local copies, waits for them, and re-layouts: 6.31 us -> none  [the longest x2 2.95 us: by_groups(): lax.all_to_all(back_b.reshape(channels, seq_len), SP, split_axis=1, conca...]
    reduce_sum x8 -> x0, other arithmetic: 3.71 us -> none  [the longest x1 1.15 us: sum_at_owner_2(): return jnp.sum(pieces, axis=0)]
  transfers between devices with their start and end apart: 7 -> 0, of which waited for: 6 -> 0; matrix products, arithmetic and copies ran while one was open for 5% -> 0% of each run, Pallas kernels for 0% -> 0%
where the time goes in v1:
time: 82.9 us; the launch traced here: 82.6 us
  Pallas kernels  73.4 us (89%)
  local copies, waits for them, and re-layouts  8.53 us (10%)
    pallas_call x1, Pallas kernels, per_device(): pl.pallas_call(kernel, out_shape=(jax.ShapeDtypeStruct((1, ROWS, WIDTH),...  73.4 us
    unnamed x16, local copies, waits for them, and re-layouts  7.31 us

profile of v1, /device:TPU:1, one launch (start us, length us, event | category | flops | bytes accessed | tf_op | source)
XLA Modules:
  0.0 82.6 jit_solution(11159253751625146005)
XLA Ops:
  0.6 0.0 copy-start.3
  0.6 0.0 copy-start.4
  0.7 0.0 copy-start.5
  0.7 1.0 %copy.16 = bf16[64,4,512]{2,0,1:T(8,128)(2,1)S(1)} copy(bf16[64,4,512]{2,1,0:T(4,128)(2,1)} %param.12) | data formatting | bytes 524288 | tf_op args[5]
  1.7 0.0 copy-done.3
  1.7 0.0 copy-done.4
  1.7 0.0 copy-done.5
  1.7 0.0 copy-start
  1.7 1.1 %copy-done = bf16[1,128,3072]{2,1,0:T(8,128)(2,1)S(1)} copy-done((bf16[1,128,3072]{2,1,0:T(8,128)(2,1)S(1)}, bf16[1,128,3072]{2,1,0:T(8,128)(2,1)}, u32[]{:S(2)}) %copy-start) | copy-done | bytes 786456
  2.8 0.0 copy-start.1
  2.8 1.1 %copy-done.1 = bf16[1,128,3072]{2,1,0:T(8,128)(2,1)S(1)} copy-done((bf16[1,128,3072]{2,1,0:T(8,128)(2,1)S(1)}, bf16[1,128,3072]{2,1,0:T(8,128)(2,1)}, u32[]{:S(2)}) %copy-start.1) | copy-done | bytes 786456
  4.0 0.0 copy-start.2
  4.0 1.1 %copy-done.2 = bf16[1,128,3072]{2,1,0:T(8,128)(2,1)S(1)} copy-done((bf16[1,128,3072]{2,1,0:T(8,128)(2,1)S(1)}, bf16[1,128,3072]{2,1,0:T(8,128)(2,1)}, u32[]{:S(2)}) %copy-start.2) | copy-done | bytes 786456
  5.1 73.4 %span.1 = (bf16[1,128,3072]{2,1,0:T(8,128)(2,1)S(1)}, bf16[1,128,3072]{2,1,0:T(8,128)(2,1)S(1)}, f32[4,64,512]{2,1,0:T(8,128)S(1)}, f32[8,8,128]{2,1,0:T(8,128)S(1)}) custom-call(bf16[1,128,3072]{2,1,0:T(8,128)(2,1)S(1)} %copy-done, bf16[1,128,3072]{2,1,0:T(8,128)(2,1)S(1)} %copy-done.1, bf16[1,128,3072]{2,1,0:T(8,128)(2,1)S(1)} %copy-done.2, ...), custom_call_target="tpu_custom_call" | custom-call | tf_op jit(solution)/shard_map/span/pallas_call | solution.py:653
  78.5 0.6 slice_bitcast_fusion
  79.1 0.6 reshape.28
  79.7 1.1 %copy.14 = f32[64,4,512]{2,1,0:T(4,128)} copy(f32[64,4,512]{2,0,1:T(8,128)S(1)} %bitcast.11) | data formatting | bytes 1048576
  80.9 0.9 %copy.19 = bf16[1,128,3072]{2,1,0:T(8,128)(2,1)} copy(bf16[1,128,3072]{2,1,0:T(8,128)(2,1)S(1)} %get-tuple-element.28) | data formatting | bytes 1572864
  81.7 0.9 %copy.20 = bf16[1,128,3072]{2,1,0:T(8,128)(2,1)} copy(bf16[1,128,3072]{2,1,0:T(8,128)(2,1)S(1)} %get-tuple-element.29) | data formatting | bytes 1572864
  (1 shorter events, 0.0 us)
Async XLA Ops:
  0.6 1.0 %copy-start.3 = (f32[3072]{0:T(1024)S(1)}, f32[3072]{0:T(1024)}, u32[]{:S(2)}) copy-start(f32[3072]{0:T(1024)} %param.10) | copy-start | bytes 36868
  0.6 1.0 %copy-start.4 = (f32[3072]{0:T(1024)S(1)}, f32[3072]{0:T(1024)}, u32[]{:S(2)}) copy-start(f32[3072]{0:T(1024)} %param.11) | copy-start | bytes 36868
  0.7 1.0 %copy-start.5 = (f32[4,512]{1,0:T(4,128)S(1)}, f32[4,512]{1,0:T(4,128)}, u32[]{:S(2)}) copy-start(f32[4,512]{1,0:T(4,128)} %bias.1) | copy-start | bytes 24580
  1.7 1.1 %copy-start = (bf16[1,128,3072]{2,1,0:T(8,128)(2,1)S(1)}, bf16[1,128,3072]{2,1,0:T(8,128)(2,1)}, u32[]{:S(2)}) copy-start(bf16[1,128,3072]{2,1,0:T(8,128)(2,1)} %gated.1) | copy-start | bytes 2359300
  2.8 1.1 %copy-start.1 = (bf16[1,128,3072]{2,1,0:T(8,128)(2,1)S(1)}, bf16[1,128,3072]{2,1,0:T(8,128)(2,1)}, u32[]{:S(2)}) copy-start(bf16[1,128,3072]{2,1,0:T(8,128)(2,1)} %values.1) | copy-start | bytes 2359300
  4.0 1.1 %copy-start.2 = (bf16[1,128,3072]{2,1,0:T(8,128)(2,1)S(1)}, bf16[1,128,3072]{2,1,0:T(8,128)(2,1)}, u32[]{:S(2)}) copy-start(bf16[1,128,3072]{2,1,0:T(8,128)(2,1)} %upstream.1) | copy-start | bytes 2359300

commit v2 on v1

v2 whole, which is shorter than its diff:
```python
import jax
import jax.numpy as jnp
from jax import lax
from jax.experimental import pallas as pl
from jax.experimental.pallas import tpu as pltpu
from jax.sharding import Mesh
from jax.sharding import PartitionSpec as P

AXES = ("z", "y", "x", "core")
DP = ("x", "core")
SP = ("z", "y")
MESH = pl.DeviceIdType.MESH
F32 = jnp.float32
BF16 = jnp.bfloat16
EPS = 1e-05

GROUPS = 4
ROWS = 128
WIDTH = 3072
CHUNKS = 8
CW = WIDTH // CHUNKS

TILES = {
    (0, 0): [(0, g) for g in range(4)],
    (1, 1): [(0, 2), (0, 3), (1, 2), (1, 3), (0, 0), (0, 1), (1, 0), (1, 1)],
    (1, 2): [(0, 2), (0, 3), (1, 2), (1, 3)],
    (1, 3): [(0, 2), (0, 3), (1, 2), (1, 3)],
    (2, 2): [(2, 0), (2, 1), (0, 0), (0, 1), (1, 0), (1, 1), (2, 2), (2, 3)],
    (2, 3): [(2, 0), (2, 1), (0, 0), (0, 1), (1, 0), (1, 1), (2, 2), (2, 3)],
    (3, 3): [(3, g) for g in range(4)],
}
FIRST = {(0, 0): 4, (1, 1): 4, (1, 2): 4, (1, 3): 4, (2, 2): 6, (2, 3): 6, (3, 3): 4}
ORDER = {0: (0, 1, 2, 3), 1: (0, 1, 2, 3), 2: (2, 3, 0, 1), 3: (2, 3, 0, 1)}
COLUMNS = {
    (0, 0): {g: (0, 128) for g in range(4)},
    (1, 1): {g: (0, 256) for g in range(4)},
    (1, 2): {2: (0, 256), 3: (0, 256)},
    (1, 3): {2: (0, 256), 3: (0, 256)},
    (2, 2): {0: (0, 384), 1: (0, 384), 2: (256, 384), 3: (256, 384)},
    (2, 3): {0: (0, 384), 1: (0, 384), 2: (256, 384), 3: (256, 384)},
    (3, 3): {g: (384, 512) for g in range(4)},
}


def remote(src, dst, send, recv, device):
    return pltpu.make_async_remote_copy(
        src_ref=src, dst_ref=dst, send_sem=send, recv_sem=recv, device_id=device, device_id_type=MESH
    )


def dot(a, b):
    return jnp.dot(a, b, preferred_element_type=F32)


def dot_t(a, b):
    return lax.dot_general(a, b, (((1,), (1,)), ((), ())), preferred_element_type=F32)


def loop(lo, hi, body, name="loop"):
    with jax.named_scope(name):
        lax.fori_loop(lo, hi, lambda i, _: (body(i), None)[1], None)


def kernel(
    gated_hbm, values_hbm, upstream_hbm, gain, shift, WT, bias,
    out_u, out_v, out_mix, out_vec, out_bias,
    gated, values, upstream,
    XC, YC, UN, MEAN, INV, RES, YP, PS1, PS2, PSQ, PR, PQ, ACC,
    WBUF, WX, WXT, BIASC, GX, GS, GR, GZ, ZR, YS, YR, ZS, ZG,
    VS, VA, VT, VB, VU, VC, VW, VD,
    in_s, w_s, f_s, w_r, w_r2, m_s, m_r, y_r, p_r, r1_s, r1_r, r2_s, r2_r, r3_s, r3_r, r4_s, r4_r,
    v_s, v_r,
):
    z, y = lax.axis_index("z"), lax.axis_index("y")
    x, core = lax.axis_index("x"), lax.axis_index("core")
    d = x * 2 + core
    half = y // 4
    j = y % 4
    up = j // 2
    inner = (j == 1) | (j == 2)
    outer = jnp.logical_not(inner)
    lower = up == 0
    upper = up == 1
    base = half * 4
    own_outer = (z, base + 3 * up, x, core)
    own_inner = (z, base + 1 + up, x, core)
    opp_inner = (z, base + 2 - up, x, core)
    opp_outer = (z, base + 3 - 3 * up, x, core)
    partner = (z, y, x, 1 - core)
    kx, ky = up, 1 - up

    def dp_peer(o):
        e = (d + o) % 8
        return e, (z, y, e // 2, e % 2)

    def z_peer(o):
        e = (z + o) % 8
        return e, (e, y, x, core)

    def y_peer(o):
        e = (y + o) % 8
        return e, (z, e, x, core)

    def phys(q):
        return (q + 4 * up) % 8

    big = ((values_hbm, values), (upstream_hbm, upstream), (gated_hbm, gated))

    def fetch(k, part):
        rows = pl.ds(part * 32, 32)
        source, dest = big[k]
        return pltpu.make_async_copy(source.at[0, rows, :], dest.at[rows, :], in_s.at[part if k == 0 else 3 + k])

    barrier = pltpu.get_barrier_semaphore()

    def greet(o):
        for peer in (dp_peer, z_peer, y_peer):
            pl.semaphore_signal(barrier, inc=1, device_id=peer(o)[1], device_id_type=MESH)

    @pl.when(lower)
    def _():
        for part in range(4):
            fetch(0, part).start()

    @pl.when(upper)
    def _():
        for part in range(4):
            fetch(1, part).start()
            fetch(2, part).start()

    loop(1, 8, greet, "greet")

    @pl.when(lower)
    def _():
        for part in range(4):
            fetch(1, part).start()
            fetch(2, part).start()

    @pl.when(upper)
    def _():
        for part in range(4):
            fetch(0, part).start()

    def stats(i):
        r = pl.multiple_of(i * 32, 32)
        fetch(0, i).wait()
        v = values[pl.ds(r, 32), :].astype(F32)
        mean = jnp.sum(v, axis=1, keepdims=True) * (1.0 / WIDTH)
        d0 = v - mean
        inv = lax.rsqrt(jnp.sum(d0 * d0, axis=1, keepdims=True) * (1.0 / WIDTH) + EPS)
        MEAN[pl.ds(r, 32), :] = jnp.broadcast_to(mean, (32, 128))
        INV[pl.ds(r, 32), :] = jnp.broadcast_to(inv, (32, 128))

    def wide(v):
        return jnp.concatenate([v] * (CW // 128), axis=1)

    def columns(c):
        return pl.ds(pl.multiple_of(c * CW, 128), CW)

    def norm(c, dest, row0):
        cols = columns(c)
        u = (values[:, cols].astype(F32) - wide(MEAN[...])) * wide(INV[...])
        UN[c] = u
        dest[c, row0 : row0 + ROWS, :] = (u * gain[:, cols] + shift[:, cols]).astype(BF16)

    def mix_grad(c, dest, row0):
        cols = columns(c)
        dest[c, row0 : row0 + ROWS, :] = (upstream[:, cols].astype(F32) * gated[:, cols].astype(F32)).astype(BF16)

    def fetched_pair():
        for k in (1, 2):
            source, dest = big[k]
            pltpu.make_async_copy(source.at[0], dest, in_s.at[3 + k]).wait()

    @pl.when(lower)
    def _():
        loop(0, 4, stats, "stats")

    @pl.when(upper)
    def _():
        fetched_pair()

    with jax.named_scope("barrier"):
        pl.semaphore_wait(barrier, 21)

    def x_near(c, to):
        return remote(XC.at[c, pl.ds(ROWS, ROWS), :], XC.at[c, pl.ds(0, ROWS), :], m_s.at[1], m_r.at[c], to)

    def x_far(c):
        return remote(
            XC.at[c, pl.ds(ROWS, ROWS), :], YC.at[c, pl.ds(2 * ROWS, ROWS), :], m_s.at[0], y_r.at[c % 4], opp_inner
        )

    def x_opp(c):
        return remote(
            XC.at[c, pl.ds(ROWS, ROWS), :], YC.at[c, pl.ds(ROWS, ROWS), :], m_s.at[0], y_r.at[c % 4], opp_inner
        )

    def p_inner(c):
        return remote(PS1.at[c], PR.at[c], m_s.at[1], p_r.at[c % 4], opp_inner)

    def p_outer(c):
        return remote(PS2.at[c], PR.at[c], m_s.at[1], p_r.at[c % 4], opp_outer)

    def q_outer(c):
        return remote(PSQ.at[c], PQ.at[c], m_s.at[0], m_r.at[c], own_outer)

    def make_x(c):
        @pl.when(lower)
        def _():
            norm(c, XC, ROWS)

        @pl.when(upper)
        def _():
            mix_grad(c, XC, ROWS)

    @pl.when(inner)
    def _():
        def send(q):
            c = phys(q)
            make_x(c)
            x_opp(c).start()

        loop(0, 4, send, "make_x")

    @pl.when(outer)
    def _():
        def send(q):
            c = phys(q + 4)
            make_x(c)
            x_near(c, own_inner).start()
            c = phys(q)
            make_x(c)
            x_far(c).start()

        loop(0, 4, send, "make_x")
        loop(0, 4, lambda q: x_near(phys(q), own_inner).start())

    def w_rows(t, g, h):
        c0, c1 = COLUMNS[t][g]
        return WBUF.at[t[1], g, pl.ds(h * 64, 64), c0:c1]

    def w_send(key, g, o):
        c0, c1 = COLUMNS[key][g]
        to = partner if o == 0 else (z, y, (x + o) % 4, core)
        land = w_r2.at[g] if o == 0 else w_r.at[key[1], g]
        return remote(WT.at[g, :, c0:c1], w_rows(key, g, core), w_s.at[0], land, to)

    for key in COLUMNS:

        @pl.when((j == key[0]) & (x == key[1]))
        def _(key=key):
            for g in ORDER[key[0]]:
                if g in COLUMNS[key]:
                    for o in (2, 1, 3, 0):
                        w_send(key, g, o).start()

    WBUF[x, :, pl.ds(pl.multiple_of(core * 64, 64), 64), :] = WT[...]

    @pl.when(inner)
    def _():
        loop(4, 8, lambda q: make_x(phys(q)), "make_x")

    @pl.when(lower)
    def _():
        fetched_pair()
        loop(0, CHUNKS, lambda c: mix_grad(c, YC, 0), "mix_grad")

    @pl.when(upper)
    def _():
        loop(0, 4, stats, "stats")
        loop(0, CHUNKS, lambda c: norm(c, YC, 0), "norm")

    VS[...] = jnp.zeros_like(VS)
    GX[...] = jnp.zeros_like(GX)
    ACC[...] = jnp.zeros_like(ACC)
    ones = jnp.ones((8, CW), BF16)
    for g in range(GROUPS):
        rows = jnp.broadcast_to(bias[pl.ds(g, 1), pl.ds(pl.multiple_of(j * 128, 128), 128)], (128, 128))
        BIASC[g] = rows.T

    def sum_bias(source, row0):
        for g in range(GROUPS):
            s = dot_t(ones, source[2 * g, pl.ds(row0, ROWS), :]) + dot_t(ones, source[2 * g + 1, pl.ds(row0, ROWS), :])
            VS[6 + g // 2, pl.ds((g % 2) * 4 + j, 1), :] = s[0:1]

    @pl.when(lower)
    def _():
        sum_bias(YC, 0)

    @pl.when(upper)
    def _():
        sum_bias(XC, ROWS)

    seg_t = lax.broadcasted_iota(jnp.int32, (128, 128), 0) // 64
    seg_s = lax.broadcasted_iota(jnp.int32, (128, 128), 1) // 64
    allowed = seg_t >= seg_s

    def tile(t, s, g):
        w = WBUF[t, g, :, s * 128 : (s + 1) * 128]
        return jnp.where(allowed, w, jnp.zeros_like(w)) if t == s else w

    def place(g, dst, src, a, b):
        WX[g, dst * 128 : (dst + 1) * 128, src * 128 : (src + 1) * 128] = a
        WXT[g, src * 128 : (src + 1) * 128, dst * 128 : (dst + 1) * 128] = b

    def w_relay(key, g):
        rows = w_rows(key, g, core)
        return remote(rows, rows, f_s.at[key[1]], w_r2.at[g], partner)

    def w_ready(jj, g):
        keys = [key for key in COLUMNS if key[0] == jj and g in COLUMNS[key]]
        with jax.named_scope("w_wait"):
            for key in keys:

                @pl.when(x != key[1])
                def _(key=key):
                    rows = w_rows(key, g, core)
                    remote(rows, rows, w_s.at[0], w_r.at[key[1], g], partner).wait_recv()
                    w_relay(key, g).start()

            c0, c1 = COLUMNS[keys[0]][g]
            rows = WBUF.at[0 : len(keys), g, 0:64, c0:c1]
            remote(rows, rows, w_s.at[0], w_r2.at[g], partner).wait_recv()
        if jj == 0:
            w = tile(0, 0, g)
            place(g, 0, 0, w, w.T)
        elif jj == 3:
            w = tile(3, 3, g)
            place(g, 0, 0, w.T, w)
        elif jj == 1:
            for t in (1, 2, 3) if g >= 2 else (1,):
                for s in (0, 1):
                    w = tile(t, s, g)
                    place(g, t - 1, s, w, w.T)
        else:
            for s in (0, 1, 2) if g < 2 else (2,):
                for t in (2, 3):
                    w = tile(t, s, g)
                    place(g, 2 - s, 3 - t, w.T, w)

    def bias_of(g, on):
        b = jnp.where(on, BIASC[g], 0.0)
        return jnp.concatenate([b] * (CW // 128), axis=1)

    def sums(c, value):
        back = value.astype(F32)
        u = UN[c]
        g = gain[:, columns(c)]
        bu = back * u
        a, b = back * g, bu * g
        ACC[0] += a[:, 0:128] + a[:, 128:256] + a[:, 256:384]
        ACC[1] += b[:, 0:128] + b[:, 128:256] + b[:, 256:384]
        gt = jnp.sum(bu, axis=0, keepdims=True)
        st = jnp.sum(back, axis=0, keepdims=True)
        for i in range(3):
            row = c * 3 + i
            VS[row // 8, pl.ds(row % 8, 1), :] = gt[:, i * 128 : (i + 1) * 128]
            VS[row // 8 + 3, pl.ds(row % 8, 1), :] = st[:, i * 128 : (i + 1) * 128]

    def put_x(c, g, value):
        value = (value + bias_of(g, lower)).astype(BF16)
        RES[kx, c] = value

        @pl.when(upper)
        def _():
            sums(c, value)

    def put_y(c, g, value):
        value = (value + bias_of(g, upper)).astype(BF16)
        RES[ky, c] = value

        @pl.when(lower)
        def _():
            sums(c, value)

    def stage(part):
        for key, tiles in TILES.items():
            jj, t = key
            lo, hi = ((0, FIRST[key]), (FIRST[key], len(tiles)))[part]
            if lo == hi:
                continue

            @pl.when(j == jj)
            def _(jj=jj, t=t, tiles=tiles, lo=lo, hi=hi):
                for index in range(lo, hi):
                    s, g = tiles[index]
                    if jj == 0:
                        value = GX[g, 0:128, 0:128]
                    elif jj == 3:
                        value = GX[g, 0:128, 0:128].T
                    elif jj == 1:
                        value = GX[g, (t - 1) * 128 : t * 128, s * 128 : (s + 1) * 128]
                    else:
                        value = GX[g, (2 - s) * 128 : (3 - s) * 128, (3 - t) * 128 : (4 - t) * 128].T
                    value = value.astype(BF16)
                    GS[t, 0, index] = value[0:64]
                    GS[t, 1, index] = value[64:128]
                for h in range(2):
                    e = 2 * t + h

                    @pl.when(d != e)
                    def _():
                        remote(
                            GS.at[t, h, lo:hi], GR.at[d, lo:hi], r1_s.at[part, t], r1_r.at[part], (z, y, t, h)
                        ).start()

                    @pl.when(d == e)
                    def _():
                        GR[e, lo:hi] = GS[t, h, lo:hi]

    def sum_dp(key, tiles):
        n = len(tiles)
        lo = FIRST[key]

        with jax.named_scope("r1_wait"):
            for part, (a, b) in enumerate(((0, lo), (lo, n))):
                if a < b:
                    there = GR.at[0:7, a:b]
                    remote(there, there, r1_s.at[0, 0], r1_r.at[part], partner).wait_recv()

        def add(i):
            total = GR[0, i].astype(F32)
            for e in range(1, 8):
                total = total + GR[e, i].astype(F32)
            total = total.astype(BF16)
            for rs in range(4):
                GZ[rs, i] = total[rs * 16 : (rs + 1) * 16]

        loop(0, n, add, "dp_add")
        m = n // 2

        def send(o):
            e, peer = z_peer(o)
            remote(GZ.at[e % 4, pl.ds((e // 4) * m, m)], ZR.at[z, 0:m], r2_s.at[0], r2_r.at[0], peer).start()

        loop(1, 8, send, "r2_send")
        ZR[z, 0:m] = GZ[z % 4, pl.ds((z // 4) * m, m)]

    def sum_z(key, tiles):
        jj = key[0]
        m = len(tiles) // 2

        with jax.named_scope("r2_wait"):
            there = ZR.at[0:7, 0:m]
            remote(there, there, r2_s.at[0], r2_r.at[0], partner).wait_recv()
        total = ZR[0, 0:m].astype(F32)
        for e in range(1, 8):
            total = total + ZR[e, 0:m].astype(F32)
        YS[0:m] = total.astype(BF16)

        def send(o):
            e, peer = y_peer(o)
            remote(YS.at[0:m], YR.at[y, 0:m], r3_s.at[0], r3_r.at[jj], peer).start()

        loop(1, 8, send, "r3_send")
        YR[y, 0:m] = YS[0:m]

    @pl.when(inner)
    def _():
        def early(c):
            s = dot(WXT[c // 2, :, 0:ROWS], YC[c, 0:ROWS, :])
            PSQ[c] = s[0:ROWS].astype(BF16)
            YP[c] = s[ROWS:]
            q_outer(c).start()

        def second(c):
            g = c // 2
            with jax.named_scope("wait_x"):
                x_near(c, own_outer).wait_recv()
            r = dot(WX[g], XC[c])
            PS1[c] = r[ROWS : 2 * ROWS].astype(BF16)
            PS2[c] = r[2 * ROWS :].astype(BF16)
            put_x(c, g, r[0:ROWS])
            p_outer(c).start()
            p_inner(c).start()
            with jax.named_scope("wait_y"):
                both_y = YC.at[c, pl.ds(ROWS, 2 * ROWS), :]
                remote(both_y, both_y, m_s.at[0], y_r.at[c % 4], opp_inner).wait_recv()
            s = dot(WXT[g], YC[c])
            PSQ[c] = s[0:ROWS].astype(BF16)
            put_y(c, g, s[ROWS:])
            q_outer(c).start()
            GX[g] += dot_t(YC[c], XC[c])

        for i in range(4):
            for jj in (1, 2):

                @pl.when(j == jj)
                def _(jj=jj, i=i):
                    w_ready(jj, ORDER[jj][i])

            if i < 2:
                loop(2 * i, 2 * i + 2, lambda q: early(phys(q)), "early")
            else:
                loop(2 * i, 2 * i + 2, lambda q: second(phys(q)), "second")

    @pl.when(inner)
    def _():
        stage(0)

        def first(q):
            c = phys(q)
            g = c // 2
            x_near(c, own_outer).wait_recv()
            put_x(c, g, dot(WX[g, 0:ROWS, :], XC[c]))
            GX[g, 0:ROWS, :] += dot_t(YC[c, 0:ROWS, :], XC[c])

        loop(0, 4, first, "first")
        stage(1)

    @pl.when(outer)
    def _():
        for jj in (0, 3):

            @pl.when(j == jj)
            def _(jj=jj):
                for g in ORDER[jj]:
                    w_ready(jj, g)

        def local(c):
            g = c // 2
            own_x = XC[c, pl.ds(ROWS, ROWS), :]
            own_y = YC[c, pl.ds(0, ROWS), :]
            put_x(c, g, dot(WX[g, 0:ROWS, 0:ROWS], own_x))
            YP[c] = dot(WXT[g, 0:ROWS, 0:ROWS], own_y)
            GX[g, 0:ROWS, 0:ROWS] += dot_t(own_y, own_x)

        loop(0, 8, local, "local")
        stage(0)

    def late_inner(q):
        c = phys(q)
        p_inner(c).wait_recv()
        put_y(c, c // 2, YP[c] + PR[c].astype(F32))

    def late_outer(q):
        c = phys(q)
        q_outer(c).wait_recv()
        p_outer(c).wait_recv()
        put_y(c, c // 2, YP[c] + PR[c].astype(F32) + PQ[c].astype(F32))

    def later_outer(q):
        c = phys(q)
        q_outer(c).wait_recv()
        put_y(c, c // 2, YP[c] + PQ[c].astype(F32))

    def owned(places, body):
        for key, tiles in TILES.items():
            if key[0] in places:

                @pl.when((j == key[0]) & (x == key[1]))
                def _(key=key, tiles=tiles):
                    body(key, tiles)

    @pl.when(inner)
    def _():
        loop(0, 3, late_inner, "late_inner")
        owned((1, 2), sum_dp)
        loop(3, 4, late_inner, "late_inner")

    def both(q):
        later_outer(q + 4)
        late_outer(q)

    @pl.when(outer)
    def _():
        owned((0, 3), sum_dp)
        loop(0, 1, both, "late_outer")
        owned((0, 3), sum_z)
        loop(1, 4, both, "late_outer")

    def vec_send(source, land, me, k, peer):
        for o in range(1, 8):
            e, to = peer(o)
            remote(source(e), land.at[me], v_s.at[k], v_r.at[k], to).start()

    def vec_wait(land, k):
        with jax.named_scope("v_wait"):
            remote(land.at[0:7], land.at[0:7], v_s.at[k], v_r.at[k], partner).wait()

    def vec_sum(land):
        total = land[0]
        for e in range(1, 8):
            total = total + land[e]
        return total

    vec_send(lambda e: VS.at[e], VA, d, 0, dp_peer)
    VA[d] = VS[d]

    @pl.when(inner)
    def _():
        owned((1, 2), sum_z)

    vec_wait(VA, 0)
    VT[...] = vec_sum(VA)
    vec_send(lambda e: VT, VB, z, 1, z_peer)
    VB[z] = VT[...]

    mean_a = jnp.sum(ACC[0], axis=1, keepdims=True) * (1.0 / WIDTH)
    mean_b = jnp.sum(ACC[1], axis=1, keepdims=True) * (1.0 / WIDTH)
    ACC[0] = jnp.broadcast_to(mean_a, (ROWS, 128))
    ACC[1] = jnp.broadcast_to(mean_b, (ROWS, 128))

    def outputs(c):
        cols = columns(c)
        scaled = RES[1, c].astype(F32) * gain[:, cols]
        out_v[0, :, cols] = (wide(INV[...]) * (scaled - wide(ACC[0]) - UN[c] * wide(ACC[1]))).astype(BF16)
        out_u[0, :, cols] = (upstream[:, cols].astype(F32) * RES[0, c].astype(F32)).astype(BF16)

    loop(0, CHUNKS, outputs, "outputs")

    vec_wait(VB, 1)
    VU[...] = vec_sum(VB)
    vec_send(lambda e: VU, VC, y, 2, y_peer)
    VC[y] = VU[...]

    for t in range(4):
        places = [(jj, tiles) for (jj, tt), tiles in TILES.items() if tt == t]
        total_tiles = sum(len(tiles) // 2 for _, tiles in places)

        @pl.when(x == t)
        def _(t=t, places=places, total_tiles=total_tiles):
            off = 0
            for jj, tiles in places:
                m = len(tiles) // 2
                for count in (1, 2):

                    @pl.when((j == jj) if count == 1 else (j != jj))
                    @jax.named_scope("r3_wait")
                    def _():
                        there = YR.at[0:count, 0:m]
                        remote(there, there, r3_s.at[0], r3_r.at[jj], partner).wait_recv()

                for i in range(m):
                    ZS[off + i] = (YR[jj, i].astype(F32) + YR[jj + 4, i].astype(F32)).astype(BF16)
                off += m

            def send(o):
                e, peer = z_peer(o)
                remote(ZS.at[0:total_tiles], ZG.at[z, 0:total_tiles], r4_s.at[0], r4_r.at[0], peer).start()

            loop(1, 8, send, "r4_send")
            ZG[z, 0:total_tiles] = ZS[0:total_tiles]

    for key in COLUMNS:

        total = sum(c1 - c0 for c0, c1 in COLUMNS[key].values())
        groups = 2 if total % 512 == 0 and key != (1, 1) and key[0] != 0 and key[0] != 3 else 4
        cols = total // groups

        @pl.when((j == key[0]) & (x == key[1]))
        def _(groups=groups, cols=cols):
            rows = WBUF.at[0:4, 0:groups, 0:64, 0:cols]
            remote(rows, rows, w_s.at[0], w_r2.at[0], partner).wait_send()

        @pl.when((j == key[0]) & (x != key[1]))
        def _(key=key, groups=groups, cols=cols):
            rows = WBUF.at[0, 0:groups, 0:64, 0:cols]
            remote(rows, rows, f_s.at[key[1]], w_r2.at[0], partner).wait_send()

    def chunks_left(source, sem):
        remote(source, source, m_s.at[sem], m_r.at[0], own_inner).wait_send()

    @pl.when(inner)
    def _():
        chunks_left(YC.at[0:4], 0)
        chunks_left(PS1, 1)

    @pl.when(outer)
    def _():
        chunks_left(PS1.at[0:4], 0)
        chunks_left(PS1, 1)

    for key, tiles in TILES.items():
        jj, t = key
        for part, (lo, hi) in enumerate(((0, FIRST[key]), (FIRST[key], len(tiles)))):
            for count in (1, 2):
                if lo < hi:

                    @pl.when((j == jj) & ((x == t) if count == 1 else (x != t)))
                    def _(t=t, count=count, lo=lo, hi=hi, part=part):
                        there = GS.at[0, 0:count, lo:hi]
                        remote(there, there, r1_s.at[part, t], r1_r.at[part], partner).wait_send()

    def sent(key, tiles):
        m = len(tiles) // 2

        there = ZR.at[0:7, 0:m]
        remote(there, there, r2_s.at[0], r2_r.at[0], partner).wait_send()
        remote(there, there, r3_s.at[0], r3_r.at[0], partner).wait_send()

    owned((0, 1, 2, 3), sent)

    vec_wait(VC, 2)
    VW[...] = vec_sum(VC)
    vec_send(lambda e: VW, VD, d, 3, dp_peer)
    VD[d] = VW[...]

    out_mix[...] = jnp.zeros_like(out_mix)
    keep = lax.broadcasted_iota(jnp.int32, (16, 128), 1) // 64 <= core
    for t in range(4):
        places = [(jj, tiles) for (jj, tt), tiles in TILES.items() if tt == t]
        total_tiles = sum(len(tiles) // 2 for _, tiles in places)

        @pl.when(x == t)
        def _(t=t, places=places, total_tiles=total_tiles):
            with jax.named_scope("r4_wait"):
                there = ZG.at[0:7, 0:total_tiles]
                remote(there, there, r4_s.at[0], r4_r.at[0], partner).wait()
            for k in range(8):
                rows = slice(16 * (k % 4), 16 * (k % 4) + 16)
                off = 0
                for jj, tiles in places:
                    m = len(tiles) // 2
                    for i in range(m):
                        s, g = tiles[(k // 4) * m + i]
                        value = ZG[k, off + i].astype(F32)
                        if s == t:
                            value = jnp.where(keep, value, 0.0)
                        out_mix[rows, g, s * 128 : (s + 1) * 128] = value
                    off += m

    vec_wait(VD, 3)
    out_vec[...] = VD[0:6]
    for g in range(GROUPS):
        for k in range(4):
            out_bias[g : g + 1, k * 128 : (k + 1) * 128] = VD[6 + g // 2, (g % 2) * 4 + k : (g % 2) * 4 + k + 1]


def writer(u, v, mix, vec, bias, out_u, out_v, out_mix, out_bias, out_gain, out_shift, sems):
    copies = [
        pltpu.make_async_copy(source, dest, sems.at[i])
        for i, (source, dest) in enumerate(
            (
                (u, out_u),
                (v, out_v),
                (mix, out_mix),
                (bias, out_bias),
                (vec.at[0:3], out_gain),
                (vec.at[3:6], out_shift),
            )
        )
    ]
    for copy in copies:
        copy.start()
    for copy in copies:
        copy.wait()


def per_device(gated, values_in, upstream, gain, shift, mix_w, mix_bias):
    vmem = pl.BlockSpec(memory_space=pltpu.VMEM)
    hbm = pl.BlockSpec(memory_space=pltpu.HBM)
    chunks = (CHUNKS, ROWS, CW)
    dma = pltpu.SemaphoreType.DMA
    results = pl.pallas_call(
        kernel,
        out_shape=(
            jax.ShapeDtypeStruct((1, ROWS, WIDTH), BF16),
            jax.ShapeDtypeStruct((1, ROWS, WIDTH), BF16),
            jax.ShapeDtypeStruct((64, GROUPS, 512), F32),
            jax.ShapeDtypeStruct((6, 8, 128), F32),
            jax.ShapeDtypeStruct((GROUPS, 512), F32),
        ),
        in_specs=[hbm] * 3 + [vmem] * 4,
        out_specs=[vmem] * 5,
        scratch_shapes=[
            pltpu.VMEM((ROWS, WIDTH), BF16),
            pltpu.VMEM((ROWS, WIDTH), BF16),
            pltpu.VMEM((ROWS, WIDTH), BF16),
            pltpu.VMEM((CHUNKS, 2 * ROWS, CW), BF16),
            pltpu.VMEM((CHUNKS, 3 * ROWS, CW), BF16),
            pltpu.VMEM(chunks, F32),
            pltpu.VMEM((ROWS, 128), F32),
            pltpu.VMEM((ROWS, 128), F32),
            pltpu.VMEM((2, *chunks), BF16),
            pltpu.VMEM(chunks, F32),
            pltpu.VMEM(chunks, BF16),
            pltpu.VMEM(chunks, BF16),
            pltpu.VMEM(chunks, BF16),
            pltpu.VMEM(chunks, BF16),
            pltpu.VMEM(chunks, BF16),
            pltpu.VMEM((2, ROWS, 128), F32),
            pltpu.VMEM((4, GROUPS, 128, 512), BF16),
            pltpu.VMEM((GROUPS, 384, 256), BF16),
            pltpu.VMEM((GROUPS, 256, 384), BF16),
            pltpu.VMEM((GROUPS, 128, 128), F32),
            pltpu.VMEM((GROUPS, 384, 256), F32),
            pltpu.VMEM((4, 2, 8, 64, 128), BF16),
            pltpu.VMEM((8, 8, 64, 128), BF16),
            pltpu.VMEM((4, 8, 16, 128), BF16),
            pltpu.VMEM((8, 4, 16, 128), BF16),
            pltpu.VMEM((4, 16, 128), BF16),
            pltpu.VMEM((8, 4, 16, 128), BF16),
            pltpu.VMEM((8, 16, 128), BF16),
            pltpu.VMEM((8, 8, 16, 128), BF16),
            pltpu.VMEM((8, 8, 128), F32),
            pltpu.VMEM((8, 8, 128), F32),
            pltpu.VMEM((8, 128), F32),
            pltpu.VMEM((8, 8, 128), F32),
            pltpu.VMEM((8, 128), F32),
            pltpu.VMEM((8, 8, 128), F32),
            pltpu.VMEM((8, 128), F32),
            pltpu.VMEM((8, 8, 128), F32),
            dma((6,)), dma((1,)), dma((4,)), dma((4, 4)), dma((4,)), dma((2,)), dma((8,)), dma((4,)), dma((4,)),
            dma((2, 4)), dma((2,)), dma((1,)), dma((1,)), dma((1,)), dma((4,)), dma((1,)), dma((1,)),
            dma((4,)), dma((4,)),
        ],
        compiler_params=pltpu.CompilerParams(
            collective_id=0, has_side_effects=True, vmem_limit_bytes=67043328 - 13312 * 1024
        ),
        name="span",
    )(
        gated,
        values_in,
        upstream,
        gain.reshape(1, WIDTH),
        shift.reshape(1, WIDTH),
        mix_w.transpose(1, 0, 2),
        mix_bias,
    )
    out_u, out_v, out_mix, out_bias, out_gain, out_shift = pl.pallas_call(
        writer,
        out_shape=(
            jax.ShapeDtypeStruct((1, ROWS, WIDTH), BF16),
            jax.ShapeDtypeStruct((1, ROWS, WIDTH), BF16),
            jax.ShapeDtypeStruct((64, GROUPS, 512), F32),
            jax.ShapeDtypeStruct((GROUPS, 512), F32),
            jax.ShapeDtypeStruct((3, 8, 128), F32),
            jax.ShapeDtypeStruct((3, 8, 128), F32),
        ),
        in_specs=[vmem] * 5,
        out_specs=[hbm] * 6,
        scratch_shapes=[dma((6,))],
        compiler_params=pltpu.CompilerParams(vmem_limit_bytes=1024 * 1024),
        name="writer",
    )(*results)
    return (out_u, out_v, out_mix, out_bias, out_gain.reshape(WIDTH), out_shift.reshape(WIDTH))


def solution(mesh):
    torus = Mesh(mesh.devices.reshape(8, 8, 4, 2), AXES)
    return jax.shard_map(
        per_device,
        mesh=torus,
        in_specs=(
            P(DP, SP, None),
            P(DP, SP, None),
            P(DP, SP, None),
            P(),
            P(),
            P(DP, None, None),
            P(),
        ),
        out_specs=(P(DP, SP, None), P(DP, SP, None), P(DP, None, None), P(), P(), P()),
        check_vma=False,
    )
```

time: 82.9 us -> 70.7 us (0.85)
  local copies, waits for them, and re-layouts: 8.53 us -> 1.03 us
  Pallas kernels: 73.4 us -> 68.8 us
    unnamed x16 -> x7, local copies, waits for them, and re-layouts: 7.31 us -> 1.03 us
    pallas_call x1, Pallas kernels: 73.4 us -> 67.5 us  [per_device(): pl.pallas_call(kernel, out_shape=(jax.ShapeDtypeStruct((1, ROWS, WIDTH),...]
    pallas_call x0 -> x1, Pallas kernels: none -> 1.37 us  [per_device(): pl.pallas_call(writer, out_shape=(jax.ShapeDtypeStruct((1, ROWS, WIDTH),...]
where the time goes in v2:
time: 70.7 us; the launch traced here: 70.6 us
  Pallas kernels  68.8 us (97%)
  local copies, waits for them, and re-layouts  1.03 us (1%)
    pallas_call x1, Pallas kernels, per_device(): pl.pallas_call(kernel, out_shape=(jax.ShapeDtypeStruct((1, ROWS, WIDTH),...  67.5 us

profile of v2, /device:TPU:1, one launch (start us, length us, event | category | flops | bytes accessed | tf_op | source)
XLA Modules:
  0.0 70.6 jit_solution(13010390358960504713)
XLA Ops:
  0.6 0.0 copy-start
  0.6 0.0 copy-start.1
  0.7 0.0 copy-start.2
  0.7 1.0 %copy.15 = bf16[64,4,512]{2,0,1:T(8,128)(2,1)S(1)} copy(bf16[64,4,512]{2,1,0:T(4,128)(2,1)} %param.12) | data formatting | bytes 524288 | tf_op args[5]
  1.7 0.0 copy-done
  1.7 0.0 copy-done.1
  1.7 0.0 copy-done.2
  1.7 67.5 %span.1 = (bf16[1,128,3072]{2,1,0:T(8,128)(2,1)S(1)}, bf16[1,128,3072]{2,1,0:T(8,128)(2,1)S(1)}, f32[64,4,512]{2,1,0:T(4,128)S(1)}, f32[6,8,128]{2,1,0:T(8,128)S(1)}, f32[4,512]{1,0:T(4,128)S(1)}) custom-call(bf16[1,128,3072]{2,1,0:T(8,128)(2,1)} %gated_hbm.1, bf16[1,128,3072]{2,1,0:T(8,128)(2,1)} %values_hbm.1, bf16[1,128,3072]{2,1,0:T(8,128)(2,1)} %upstream_hbm.1, ...), custom_call_target="tpu_custom_call" | custom-call | tf_op jit(solution)/shard_map/span/pallas_call | solution.py:756
  69.2 1.4 %writer.1 = (bf16[1,128,3072]{2,1,0:T(8,128)(2,1)}, bf16[1,128,3072]{2,1,0:T(8,128)(2,1)}, f32[64,4,512]{2,1,0:T(4,128)}, f32[4,512]{1,0:T(4,128)}, f32[3,8,128]{2,1,0:T(8,128)}, /*index=5*/f32[3,8,128]{2,1,0:T(8,128)}) custom-call(bf16[1,128,3072]{2,1,0:T(8,128)(2,1)S(1)} %get-tuple-element.17.u, bf16[1,128,3072]{2,1,0:T(8,128)(2,1)S(1)} %get-tuple-element.18.v, ...), custom_call_target="tpu_custom_call" | custom-call | tf_op jit(solution)/shard_map/writer/pallas_call | solution.py:822
Async XLA Ops:
  0.6 1.0 %copy-start = (f32[3072]{0:T(1024)S(1)}, f32[3072]{0:T(1024)}, u32[]{:S(2)}) copy-start(f32[3072]{0:T(1024)} %param.10) | copy-start | bytes 36868
  0.6 1.0 %copy-start.1 = (f32[3072]{0:T(1024)S(1)}, f32[3072]{0:T(1024)}, u32[]{:S(2)}) copy-start(f32[3072]{0:T(1024)} %param.11) | copy-start | bytes 36868
  0.7 1.0 %copy-start.2 = (f32[4,512]{1,0:T(4,128)S(1)}, f32[4,512]{1,0:T(4,128)}, u32[]{:S(2)}) copy-start(f32[4,512]{1,0:T(4,128)} %bias.1) | copy-start | bytes 24580

commit v3 on v2

--- a/solution.py
+++ b/solution.py
@@ -65,7 +65,7 @@
     gated_hbm, values_hbm, upstream_hbm, gain, shift, WT, bias,
     out_u, out_v, out_mix, out_vec, out_bias,
     gated, values, upstream,
-    XC, YC, UN, MEAN, INV, RES, YP, PS1, PS2, PSQ, PR, PQ, ACC,
+    XC, XF, YC, UN, MEAN, INV, RES, YP, PS1, PS2, PSQ, PR, PQ, ACC,
     WBUF, WX, WXT, BIASC, GX, GS, GR, GZ, ZR, YS, YR, ZS, ZG,
     VS, VA, VT, VB, VU, VC, VW, VD,
     in_s, w_s, f_s, w_r, w_r2, m_s, m_r, y_r, p_r, r1_s, r1_r, r2_s, r2_r, r3_s, r3_r, r4_s, r4_r,
@@ -157,15 +157,20 @@
     def columns(c):
         return pl.ds(pl.multiple_of(c * CW, 128), CW)
 
-    def norm(c, dest, row0):
+    def norm(c, dest, row0, far=False):
         cols = columns(c)
         u = (values[:, cols].astype(F32) - wide(MEAN[...])) * wide(INV[...])
         UN[c] = u
+        if far:
+            XF[c % 4] = u.astype(BF16)
         dest[c, row0 : row0 + ROWS, :] = (u * gain[:, cols] + shift[:, cols]).astype(BF16)
 
-    def mix_grad(c, dest, row0):
+    def mix_grad(c, dest, row0, far=False):
         cols = columns(c)
-        dest[c, row0 : row0 + ROWS, :] = (upstream[:, cols].astype(F32) * gated[:, cols].astype(F32)).astype(BF16)
+        m = (upstream[:, cols].astype(F32) * gated[:, cols].astype(F32)).astype(BF16)
+        if far:
+            XF[c % 4] = m
+        dest[c, row0 : row0 + ROWS, :] = m
 
     def fetched_pair():
         for k in (1, 2):
@@ -188,12 +193,12 @@
 
     def x_far(c):
         return remote(
-            XC.at[c, pl.ds(ROWS, ROWS), :], YC.at[c, pl.ds(2 * ROWS, ROWS), :], m_s.at[0], y_r.at[c % 4], opp_inner
+            XF.at[c % 4], YC.at[c, pl.ds(2 * ROWS, ROWS), :], m_s.at[0], y_r.at[c % 4], opp_inner
         )
 
     def x_opp(c):
         return remote(
-            XC.at[c, pl.ds(ROWS, ROWS), :], YC.at[c, pl.ds(ROWS, ROWS), :], m_s.at[0], y_r.at[c % 4], opp_inner
+            XF.at[c % 4], YC.at[c, pl.ds(ROWS, ROWS), :], m_s.at[0], y_r.at[c % 4], opp_inner
         )
 
     def p_inner(c):
@@ -205,20 +210,20 @@
     def q_outer(c):
         return remote(PSQ.at[c], PQ.at[c], m_s.at[0], m_r.at[c], own_outer)
 
-    def make_x(c):
+    def make_x(c, far):
         @pl.when(lower)
         def _():
-            norm(c, XC, ROWS)
+            norm(c, XC, ROWS, far)
 
         @pl.when(upper)
         def _():
-            mix_grad(c, XC, ROWS)
+            mix_grad(c, XC, ROWS, far)
 
     @pl.when(inner)
     def _():
         def send(q):
             c = phys(q)
-            make_x(c)
+            make_x(c, True)
             x_opp(c).start()
 
         loop(0, 4, send, "make_x")
@@ -227,10 +232,10 @@
     def _():
         def send(q):
             c = phys(q + 4)
-            make_x(c)
+            make_x(c, False)
             x_near(c, own_inner).start()
             c = phys(q)
-            make_x(c)
+            make_x(c, True)
             x_far(c).start()
 
         loop(0, 4, send, "make_x")
@@ -259,7 +264,7 @@
 
     @pl.when(inner)
     def _():
-        loop(4, 8, lambda q: make_x(phys(q)), "make_x")
+        loop(4, 8, lambda q: make_x(phys(q), False), "make_x")
 
     @pl.when(lower)
     def _():
@@ -343,20 +348,19 @@
         b = jnp.where(on, BIASC[g], 0.0)
         return jnp.concatenate([b] * (CW // 128), axis=1)
 
-    def sums(c, value):
-        back = value.astype(F32)
-        u = UN[c]
-        g = gain[:, columns(c)]
-        bu = back * u
-        a, b = back * g, bu * g
+    def row_sums(c, back):
+        a = back * gain[:, columns(c)]
+        b = a * UN[c]
         ACC[0] += a[:, 0:128] + a[:, 128:256] + a[:, 256:384]
         ACC[1] += b[:, 0:128] + b[:, 128:256] + b[:, 256:384]
-        gt = jnp.sum(bu, axis=0, keepdims=True)
+
+    def column_sums(c, product, back):
+        gt = jnp.sum(product, axis=0, keepdims=True)
         st = jnp.sum(back, axis=0, keepdims=True)
         for i in range(3):
             row = c * 3 + i
-            VS[row // 8, pl.ds(row % 8, 1), :] = gt[:, i * 128 : (i + 1) * 128]
-            VS[row // 8 + 3, pl.ds(row % 8, 1), :] = st[:, i * 128 : (i + 1) * 128]
+            VS[row // 8, pl.ds(row % 8, 1), :] += gt[:, i * 128 : (i + 1) * 128]
+            VS[row // 8 + 3, pl.ds(row % 8, 1), :] += st[:, i * 128 : (i + 1) * 128]
 
     def put_x(c, g, value):
         value = (value + bias_of(g, lower)).astype(BF16)
@@ -364,15 +368,20 @@
 
         @pl.when(upper)
         def _():
-            sums(c, value)
-
-    def put_y(c, g, value):
+            back = value.astype(F32)
+            row_sums(c, back)
+            column_sums(c, back * UN[c], back)
+
+    def put_y(c, g, value, columns_too):
         value = (value + bias_of(g, upper)).astype(BF16)
         RES[ky, c] = value
 
         @pl.when(lower)
         def _():
-            sums(c, value)
+            back = value.astype(F32)
+            row_sums(c, back)
+            if columns_too:
+                column_sums(c, back * UN[c], back)
 
     def stage(part):
         for key, tiles in TILES.items():
@@ -464,6 +473,10 @@
             YP[c] = s[ROWS:]
             q_outer(c).start()
 
+            @pl.when(lower)
+            def _():
+                column_sums(c, s[ROWS:] * UN[c], s[ROWS:])
+
         def second(c):
             g = c // 2
             with jax.named_scope("wait_x"):
@@ -477,10 +490,18 @@
             with jax.named_scope("wait_y"):
                 both_y = YC.at[c, pl.ds(ROWS, 2 * ROWS), :]
                 remote(both_y, both_y, m_s.at[0], y_r.at[c % 4], opp_inner).wait_recv()
+
+            @pl.when(upper)
+            def _():
+                u = YC[c, pl.ds(ROWS, 2 * ROWS), :].astype(F32)
+                near, far = PS1[c].astype(F32), PS2[c].astype(F32)
+                column_sums(c, near * u[0:ROWS] + far * u[ROWS:], near + far)
+                YC[c, pl.ds(ROWS, 2 * ROWS), :] = (u * gain[:, columns(c)] + shift[:, columns(c)]).astype(BF16)
+
             s = dot(WXT[g], YC[c])
             PSQ[c] = s[0:ROWS].astype(BF16)
-            put_y(c, g, s[ROWS:])
             q_outer(c).start()
+            put_y(c, g, s[ROWS:], True)
             GX[g] += dot_t(YC[c], XC[c])
 
         for i in range(4):
@@ -507,7 +528,6 @@
             GX[g, 0:ROWS, :] += dot_t(YC[c, 0:ROWS, :], XC[c])
 
         loop(0, 4, first, "first")
-        stage(1)
 
     @pl.when(outer)
     def _():
@@ -529,21 +549,25 @@
         loop(0, 8, local, "local")
         stage(0)
 
-    def late_inner(q):
+    def late(q):
         c = phys(q)
         p_inner(c).wait_recv()
-        put_y(c, c // 2, YP[c] + PR[c].astype(F32))
-
-    def late_outer(q):
+        put_y(c, c // 2, YP[c] + PR[c].astype(F32), False)
+
+    def near_part(q):
         c = phys(q)
         q_outer(c).wait_recv()
-        p_outer(c).wait_recv()
-        put_y(c, c // 2, YP[c] + PR[c].astype(F32) + PQ[c].astype(F32))
-
-    def later_outer(q):
+        part = YP[c] + PQ[c].astype(F32)
+        YP[c] = part
+
+        @pl.when(lower)
+        def _():
+            column_sums(c, part * UN[c], part)
+
+    def near_whole(q):
         c = phys(q)
         q_outer(c).wait_recv()
-        put_y(c, c // 2, YP[c] + PQ[c].astype(F32))
+        put_y(c, c // 2, YP[c] + PQ[c].astype(F32), True)
 
     def owned(places, body):
         for key, tiles in TILES.items():
@@ -553,22 +577,13 @@
                 def _(key=key, tiles=tiles):
                     body(key, tiles)
 
-    @pl.when(inner)
-    def _():
-        loop(0, 3, late_inner, "late_inner")
-        owned((1, 2), sum_dp)
-        loop(3, 4, late_inner, "late_inner")
-
-    def both(q):
-        later_outer(q + 4)
-        late_outer(q)
-
     @pl.when(outer)
     def _():
+        loop(0, 4, near_part, "near_part")
         owned((0, 3), sum_dp)
-        loop(0, 1, both, "late_outer")
+        loop(4, 6, near_whole, "near_whole")
         owned((0, 3), sum_z)
-        loop(1, 4, both, "late_outer")
+        loop(6, 8, near_whole, "near_whole")
 
     def vec_send(source, land, me, k, peer):
         for o in range(1, 8):
@@ -590,12 +605,29 @@
 
     @pl.when(inner)
     def _():
-        owned((1, 2), sum_z)
-
+        stage(1)
+
+    late(0)
     vec_wait(VA, 0)
     VT[...] = vec_sum(VA)
     vec_send(lambda e: VT, VB, z, 1, z_peer)
     VB[z] = VT[...]
+    late(1)
+
+    @pl.when(inner)
+    def _():
+        owned((1, 2), sum_dp)
+
+    late(2)
+    vec_wait(VB, 1)
+    VU[...] = vec_sum(VB)
+    vec_send(lambda e: VU, VC, y, 2, y_peer)
+    VC[y] = VU[...]
+    late(3)
+
+    @pl.when(inner)
+    def _():
+        owned((1, 2), sum_z)
 
     mean_a = jnp.sum(ACC[0], axis=1, keepdims=True) * (1.0 / WIDTH)
     mean_b = jnp.sum(ACC[1], axis=1, keepdims=True) * (1.0 / WIDTH)
@@ -610,10 +642,10 @@
 
     loop(0, CHUNKS, outputs, "outputs")
 
-    vec_wait(VB, 1)
-    VU[...] = vec_sum(VB)
-    vec_send(lambda e: VU, VC, y, 2, y_peer)
-    VC[y] = VU[...]
+    vec_wait(VC, 2)
+    VW[...] = vec_sum(VC)
+    vec_send(lambda e: VW, VD, d, 3, dp_peer)
+    VD[d] = VW[...]
 
     for t in range(4):
         places = [(jj, tiles) for (jj, tt), tiles in TILES.items() if tt == t]
@@ -691,11 +723,6 @@
         remote(there, there, r3_s.at[0], r3_r.at[0], partner).wait_send()
 
     owned((0, 1, 2, 3), sent)
-
-    vec_wait(VC, 2)
-    VW[...] = vec_sum(VC)
-    vec_send(lambda e: VW, VD, d, 3, dp_peer)
-    VD[d] = VW[...]
 
     out_mix[...] = jnp.zeros_like(out_mix)
     keep = lax.broadcasted_iota(jnp.int32, (16, 128), 1) // 64 <= core
@@ -769,6 +796,7 @@
             pltpu.VMEM((ROWS, WIDTH), BF16),
             pltpu.VMEM((ROWS, WIDTH), BF16),
             pltpu.VMEM((CHUNKS, 2 * ROWS, CW), BF16),
+            pltpu.VMEM((CHUNKS // 2, ROWS, CW), BF16),
             pltpu.VMEM((CHUNKS, 3 * ROWS, CW), BF16),
             pltpu.VMEM(chunks, F32),
             pltpu.VMEM((ROWS, 128), F32),

time: 70.7 us -> 68.1 us (0.963)
  the two profiles are of different devices: /device:TPU:1 before, /device:TPU:2 now
where the time goes in v3:
time: 68.1 us; the launch traced here: 67.9 us
  Pallas kernels  66.2 us (97%)
  local copies, waits for them, and re-layouts  1.03 us (2%)
  between operations  0.69 us (1%)
    pallas_call x1, Pallas kernels, per_device(): pl.pallas_call(kernel, out_shape=(jax.ShapeDtypeStruct((1, ROWS, WIDTH),...  64.9 us
    pallas_call x1, Pallas kernels, per_device(): pl.pallas_call(writer, out_shape=(jax.ShapeDtypeStruct((1, ROWS, WIDTH),...  1.37 us

profile of v3, /device:TPU:2, one launch (start us, length us, event | category | flops | bytes accessed | tf_op | source)
XLA Modules:
  0.0 67.9 jit_solution(13724542572078940113)
XLA Ops:
  0.6 0.0 copy-start
  0.6 0.0 copy-start.1
  0.7 0.0 copy-start.2
  0.7 1.0 %copy.15 = bf16[64,4,512]{2,0,1:T(8,128)(2,1)S(1)} copy(bf16[64,4,512]{2,1,0:T(4,128)(2,1)} %param.12) | data formatting | bytes 524288 | tf_op args[5]
  1.7 0.0 copy-done
  1.7 0.0 copy-done.1
  1.7 0.0 copy-done.2
  1.7 64.9 %span.1 = (bf16[1,128,3072]{2,1,0:T(8,128)(2,1)S(1)}, bf16[1,128,3072]{2,1,0:T(8,128)(2,1)S(1)}, f32[64,4,512]{2,1,0:T(4,128)S(1)}, f32[6,8,128]{2,1,0:T(8,128)S(1)}, f32[4,512]{1,0:T(4,128)S(1)}) custom-call(bf16[1,128,3072]{2,1,0:T(8,128)(2,1)} %gated_hbm.1, bf16[1,128,3072]{2,1,0:T(8,128)(2,1)} %values_hbm.1, bf16[1,128,3072]{2,1,0:T(8,128)(2,1)} %upstream_hbm.1, ...), custom_call_target="tpu_custom_call" | custom-call | tf_op jit(solution)/shard_map/span/pallas_call | solution.py:783
  66.6 1.4 %writer.1 = (bf16[1,128,3072]{2,1,0:T(8,128)(2,1)}, bf16[1,128,3072]{2,1,0:T(8,128)(2,1)}, f32[64,4,512]{2,1,0:T(4,128)}, f32[4,512]{1,0:T(4,128)}, f32[3,8,128]{2,1,0:T(8,128)}, /*index=5*/f32[3,8,128]{2,1,0:T(8,128)}) custom-call(bf16[1,128,3072]{2,1,0:T(8,128)(2,1)S(1)} %get-tuple-element.17.u, bf16[1,128,3072]{2,1,0:T(8,128)(2,1)S(1)} %get-tuple-element.18.v, ...), custom_call_target="tpu_custom_call" | custom-call | tf_op jit(solution)/shard_map/writer/pallas_call | solution.py:850
Async XLA Ops:
  0.6 1.0 %copy-start = (f32[3072]{0:T(1024)S(1)}, f32[3072]{0:T(1024)}, u32[]{:S(2)}) copy-start(f32[3072]{0:T(1024)} %param.10) | copy-start | bytes 36868
  0.6 1.0 %copy-start.1 = (f32[3072]{0:T(1024)S(1)}, f32[3072]{0:T(1024)}, u32[]{:S(2)}) copy-start(f32[3072]{0:T(1024)} %param.11) | copy-start | bytes 36868
  0.7 1.0 %copy-start.2 = (f32[4,512]{1,0:T(4,128)S(1)}, f32[4,512]{1,0:T(4,128)}, u32[]{:S(2)}) copy-start(f32[4,512]{1,0:T(4,128)} %bias.1) | copy-start | bytes 24580

commit v4 on v3

--- a/solution.py
+++ b/solution.py
@@ -22,14 +22,22 @@
 
 TILES = {
     (0, 0): [(0, g) for g in range(4)],
-    (1, 1): [(0, 2), (0, 3), (1, 2), (1, 3), (0, 0), (0, 1), (1, 0), (1, 1)],
-    (1, 2): [(0, 2), (0, 3), (1, 2), (1, 3)],
-    (1, 3): [(0, 2), (0, 3), (1, 2), (1, 3)],
-    (2, 2): [(2, 0), (2, 1), (0, 0), (0, 1), (1, 0), (1, 1), (2, 2), (2, 3)],
-    (2, 3): [(2, 0), (2, 1), (0, 0), (0, 1), (1, 0), (1, 1), (2, 2), (2, 3)],
+    (1, 1): [(0, 0), (0, 1), (1, 0), (1, 1), (0, 2), (1, 2), (0, 3), (1, 3)],
+    (1, 2): [(0, 2), (1, 2), (0, 3), (1, 3)],
+    (1, 3): [(0, 2), (1, 2), (0, 3), (1, 3)],
+    (2, 2): [(2, 2), (2, 3), (2, 0), (0, 0), (1, 0), (2, 1), (0, 1), (1, 1)],
+    (2, 3): [(2, 2), (2, 3), (2, 0), (0, 0), (1, 0), (2, 1), (0, 1), (1, 1)],
     (3, 3): [(3, g) for g in range(4)],
 }
-FIRST = {(0, 0): 4, (1, 1): 4, (1, 2): 4, (1, 3): 4, (2, 2): 6, (2, 3): 6, (3, 3): 4}
+ENDS = {
+    (0, 0): (0, 4, 4, 4),
+    (1, 1): (0, 4, 6, 8),
+    (1, 2): (0, 0, 2, 4),
+    (1, 3): (0, 0, 2, 4),
+    (2, 2): (0, 2, 5, 8),
+    (2, 3): (0, 2, 5, 8),
+    (3, 3): (0, 4, 4, 4),
+}
 ORDER = {0: (0, 1, 2, 3), 1: (0, 1, 2, 3), 2: (2, 3, 0, 1), 3: (2, 3, 0, 1)}
 COLUMNS = {
     (0, 0): {g: (0, 128) for g in range(4)},
@@ -65,7 +73,7 @@
     gated_hbm, values_hbm, upstream_hbm, gain, shift, WT, bias,
     out_u, out_v, out_mix, out_vec, out_bias,
     gated, values, upstream,
-    XC, XF, YC, UN, MEAN, INV, RES, YP, PS1, PS2, PSQ, PR, PQ, ACC,
+    XC, XF, XR, YC, UN, MEAN, INV, RES, YP, PS1, PS2, PSQ, PR, PQ, ACC,
     WBUF, WX, WXT, BIASC, GX, GS, GR, GZ, ZR, YS, YR, ZS, ZG,
     VS, VA, VT, VB, VU, VC, VW, VD,
     in_s, w_s, f_s, w_r, w_r2, m_s, m_r, y_r, p_r, r1_s, r1_r, r2_s, r2_r, r3_s, r3_r, r4_s, r4_r,
@@ -162,14 +170,14 @@
         u = (values[:, cols].astype(F32) - wide(MEAN[...])) * wide(INV[...])
         UN[c] = u
         if far:
-            XF[c % 4] = u.astype(BF16)
+            XF[c] = u.astype(BF16)
         dest[c, row0 : row0 + ROWS, :] = (u * gain[:, cols] + shift[:, cols]).astype(BF16)
 
     def mix_grad(c, dest, row0, far=False):
         cols = columns(c)
         m = (upstream[:, cols].astype(F32) * gated[:, cols].astype(F32)).astype(BF16)
         if far:
-            XF[c % 4] = m
+            XF[c] = m
         dest[c, row0 : row0 + ROWS, :] = m
 
     def fetched_pair():
@@ -188,18 +196,14 @@
     with jax.named_scope("barrier"):
         pl.semaphore_wait(barrier, 21)
 
-    def x_near(c, to):
-        return remote(XC.at[c, pl.ds(ROWS, ROWS), :], XC.at[c, pl.ds(0, ROWS), :], m_s.at[1], m_r.at[c], to)
-
-    def x_far(c):
-        return remote(
-            XF.at[c % 4], YC.at[c, pl.ds(2 * ROWS, ROWS), :], m_s.at[0], y_r.at[c % 4], opp_inner
-        )
+    def x_near(c):
+        return remote(XF.at[c], XR.at[c], m_s.at[1], m_r.at[c], own_inner)
 
     def x_opp(c):
-        return remote(
-            XF.at[c % 4], YC.at[c, pl.ds(ROWS, ROWS), :], m_s.at[0], y_r.at[c % 4], opp_inner
-        )
+        return remote(XF.at[c], YC.at[c, pl.ds(ROWS, ROWS), :], m_s.at[0], y_r.at[c % 4], opp_inner)
+
+    def x_relay(c):
+        return remote(XR.at[c], YC.at[c, pl.ds(2 * ROWS, ROWS), :], m_s.at[1], y_r.at[c % 4], opp_inner)
 
     def p_inner(c):
         return remote(PS1.at[c], PR.at[c], m_s.at[1], p_r.at[c % 4], opp_inner)
@@ -210,20 +214,20 @@
     def q_outer(c):
         return remote(PSQ.at[c], PQ.at[c], m_s.at[0], m_r.at[c], own_outer)
 
-    def make_x(c, far):
+    def make_x(c):
         @pl.when(lower)
         def _():
-            norm(c, XC, ROWS, far)
+            norm(c, XC, ROWS, True)
 
         @pl.when(upper)
         def _():
-            mix_grad(c, XC, ROWS, far)
+            mix_grad(c, XC, ROWS, True)
 
     @pl.when(inner)
     def _():
         def send(q):
             c = phys(q)
-            make_x(c, True)
+            make_x(c)
             x_opp(c).start()
 
         loop(0, 4, send, "make_x")
@@ -231,15 +235,11 @@
     @pl.when(outer)
     def _():
         def send(q):
-            c = phys(q + 4)
-            make_x(c, False)
-            x_near(c, own_inner).start()
             c = phys(q)
-            make_x(c, True)
-            x_far(c).start()
-
-        loop(0, 4, send, "make_x")
-        loop(0, 4, lambda q: x_near(phys(q), own_inner).start())
+            make_x(c)
+            x_near(c).start()
+
+        loop(0, 8, send, "make_x")
 
     def w_rows(t, g, h):
         c0, c1 = COLUMNS[t][g]
@@ -264,7 +264,7 @@
 
     @pl.when(inner)
     def _():
-        loop(4, 8, lambda q: make_x(phys(q), False), "make_x")
+        loop(4, 8, lambda q: make_x(phys(q)), "make_x")
 
     @pl.when(lower)
     def _():
@@ -386,7 +386,7 @@
     def stage(part):
         for key, tiles in TILES.items():
             jj, t = key
-            lo, hi = ((0, FIRST[key]), (FIRST[key], len(tiles)))[part]
+            lo, hi = ENDS[key][part : part + 2]
             if lo == hi:
                 continue
 
@@ -420,10 +420,9 @@
 
     def sum_dp(key, tiles):
         n = len(tiles)
-        lo = FIRST[key]
-
         with jax.named_scope("r1_wait"):
-            for part, (a, b) in enumerate(((0, lo), (lo, n))):
+            for part in range(3):
+                a, b = ENDS[key][part : part + 2]
                 if a < b:
                     there = GR.at[0:7, a:b]
                     remote(there, there, r1_s.at[0, 0], r1_r.at[part], partner).wait_recv()
@@ -467,8 +466,26 @@
 
     @pl.when(inner)
     def _():
-        def early(c):
-            s = dot(WXT[c // 2, :, 0:ROWS], YC[c, 0:ROWS, :])
+        def arrived(c):
+            x_near(c).wait_recv()
+
+        def take(c):
+            @pl.when(lower)
+            def _():
+                n = XR[c].astype(F32) * gain[:, columns(c)] + shift[:, columns(c)]
+                XC[c, pl.ds(0, ROWS), :] = n.astype(BF16)
+
+            @pl.when(upper)
+            def _():
+                XC[c, pl.ds(0, ROWS), :] = XR[c]
+
+        def outer_sums(c):
+            back = PSQ[c].astype(F32)
+            column_sums(c, back * XR[c].astype(F32), back)
+
+        def first(c):
+            g = c // 2
+            s = dot(WXT[g, :, 0:ROWS], YC[c, 0:ROWS, :])
             PSQ[c] = s[0:ROWS].astype(BF16)
             YP[c] = s[ROWS:]
             q_outer(c).start()
@@ -477,16 +494,28 @@
             def _():
                 column_sums(c, s[ROWS:] * UN[c], s[ROWS:])
 
+            with jax.named_scope("wait_x"):
+                arrived(c)
+            x_relay(c).start()
+            take(c)
+            put_x(c, g, dot(WX[g, 0:ROWS, :], XC[c]))
+            GX[g, 0:ROWS, :] += dot_t(YC[c, 0:ROWS, :], XC[c])
+
+            @pl.when(lower)
+            def _():
+                outer_sums(c)
+
         def second(c):
             g = c // 2
             with jax.named_scope("wait_x"):
-                x_near(c, own_outer).wait_recv()
+                arrived(c)
+            take(c)
             r = dot(WX[g], XC[c])
             PS1[c] = r[ROWS : 2 * ROWS].astype(BF16)
             PS2[c] = r[2 * ROWS :].astype(BF16)
-            put_x(c, g, r[0:ROWS])
             p_outer(c).start()
             p_inner(c).start()
+            put_x(c, g, r[0:ROWS])
             with jax.named_scope("wait_y"):
                 both_y = YC.at[c, pl.ds(ROWS, 2 * ROWS), :]
                 remote(both_y, both_y, m_s.at[0], y_r.at[c % 4], opp_inner).wait_recv()
@@ -500,9 +529,13 @@
 
             s = dot(WXT[g], YC[c])
             PSQ[c] = s[0:ROWS].astype(BF16)
+            put_y(c, g, s[ROWS:], True)
             q_outer(c).start()
-            put_y(c, g, s[ROWS:], True)
             GX[g] += dot_t(YC[c], XC[c])
+
+            @pl.when(lower)
+            def _():
+                outer_sums(c)
 
         for i in range(4):
             for jj in (1, 2):
@@ -512,22 +545,12 @@
                     w_ready(jj, ORDER[jj][i])
 
             if i < 2:
-                loop(2 * i, 2 * i + 2, lambda q: early(phys(q)), "early")
+                loop(2 * i, 2 * i + 2, lambda q: first(phys(q)), "first")
             else:
                 loop(2 * i, 2 * i + 2, lambda q: second(phys(q)), "second")
-
-    @pl.when(inner)
-    def _():
-        stage(0)
-
-        def first(q):
-            c = phys(q)
-            g = c // 2
-            x_near(c, own_outer).wait_recv()
-            put_x(c, g, dot(WX[g, 0:ROWS, :], XC[c]))
-            GX[g, 0:ROWS, :] += dot_t(YC[c, 0:ROWS, :], XC[c])
-
-        loop(0, 4, first, "first")
+            if i > 0:
+                with jax.named_scope("stage"):
+                    stage(i - 1)
 
     @pl.when(outer)
     def _():
@@ -543,7 +566,13 @@
             own_x = XC[c, pl.ds(ROWS, ROWS), :]
             own_y = YC[c, pl.ds(0, ROWS), :]
             put_x(c, g, dot(WX[g, 0:ROWS, 0:ROWS], own_x))
-            YP[c] = dot(WXT[g, 0:ROWS, 0:ROWS], own_y)
+            part = dot(WXT[g, 0:ROWS, 0:ROWS], own_y)
+            YP[c] = part
+
+            @pl.when(lower)
+            def _():
+                column_sums(c, part * UN[c], part)
+
             GX[g, 0:ROWS, 0:ROWS] += dot_t(own_y, own_x)
 
         loop(0, 8, local, "local")
@@ -557,17 +586,12 @@
     def near_part(q):
         c = phys(q)
         q_outer(c).wait_recv()
-        part = YP[c] + PQ[c].astype(F32)
-        YP[c] = part
-
-        @pl.when(lower)
-        def _():
-            column_sums(c, part * UN[c], part)
+        YP[c] += PQ[c].astype(F32)
 
     def near_whole(q):
         c = phys(q)
         q_outer(c).wait_recv()
-        put_y(c, c // 2, YP[c] + PQ[c].astype(F32), True)
+        put_y(c, c // 2, YP[c] + PQ[c].astype(F32), False)
 
     def owned(places, body):
         for key, tiles in TILES.items():
@@ -576,14 +600,6 @@
                 @pl.when((j == key[0]) & (x == key[1]))
                 def _(key=key, tiles=tiles):
                     body(key, tiles)
-
-    @pl.when(outer)
-    def _():
-        loop(0, 4, near_part, "near_part")
-        owned((0, 3), sum_dp)
-        loop(4, 6, near_whole, "near_whole")
-        owned((0, 3), sum_z)
-        loop(6, 8, near_whole, "near_whole")
 
     def vec_send(source, land, me, k, peer):
         for o in range(1, 8):
@@ -600,34 +616,51 @@
             total = total + land[e]
         return total
 
-    vec_send(lambda e: VS.at[e], VA, d, 0, dp_peer)
-    VA[d] = VS[d]
+    def vec_dp():
+        vec_send(lambda e: VS.at[e], VA, d, 0, dp_peer)
+        VA[d] = VS[d]
+
+    def vec_z():
+        vec_wait(VA, 0)
+        VT[...] = vec_sum(VA)
+        vec_send(lambda e: VT, VB, z, 1, z_peer)
+        VB[z] = VT[...]
+
+    def vec_y():
+        vec_wait(VB, 1)
+        VU[...] = vec_sum(VB)
+        vec_send(lambda e: VU, VC, y, 2, y_peer)
+        VC[y] = VU[...]
 
     @pl.when(inner)
     def _():
-        stage(1)
-
-    late(0)
-    vec_wait(VA, 0)
-    VT[...] = vec_sum(VA)
-    vec_send(lambda e: VT, VB, z, 1, z_peer)
-    VB[z] = VT[...]
-    late(1)
-
-    @pl.when(inner)
-    def _():
+        vec_dp()
+        late(0)
+        vec_z()
+        late(1)
         owned((1, 2), sum_dp)
-
-    late(2)
-    vec_wait(VB, 1)
-    VU[...] = vec_sum(VB)
-    vec_send(lambda e: VU, VC, y, 2, y_peer)
-    VC[y] = VU[...]
-    late(3)
-
-    @pl.when(inner)
-    def _():
+        vec_y()
+        late(2)
         owned((1, 2), sum_z)
+
+    @pl.when(outer)
+    def _():
+        vec_dp()
+        owned((0, 3), sum_dp)
+        loop(0, 4, near_part, "near_part")
+        owned((0, 3), sum_z)
+        vec_z()
+        loop(4, 6, near_whole, "near_whole")
+        vec_y()
+        loop(6, 8, near_whole, "near_whole")
+        loop(0, 3, late, "late")
+
+    vec_wait(VC, 2)
+    VW[...] = vec_sum(VC)
+    vec_send(lambda e: VW, VD, d, 3, dp_peer)
+    VD[d] = VW[...]
+    with jax.named_scope("late"):
+        late(3)
 
     mean_a = jnp.sum(ACC[0], axis=1, keepdims=True) * (1.0 / WIDTH)
     mean_b = jnp.sum(ACC[1], axis=1, keepdims=True) * (1.0 / WIDTH)
@@ -641,11 +674,6 @@
         out_u[0, :, cols] = (upstream[:, cols].astype(F32) * RES[0, c].astype(F32)).astype(BF16)
 
     loop(0, CHUNKS, outputs, "outputs")
-
-    vec_wait(VC, 2)
-    VW[...] = vec_sum(VC)
-    vec_send(lambda e: VW, VD, d, 3, dp_peer)
-    VD[d] = VW[...]
 
     for t in range(4):
         places = [(jj, tiles) for (jj, tt), tiles in TILES.items() if tt == t]
@@ -697,16 +725,16 @@
     @pl.when(inner)
     def _():
         chunks_left(YC.at[0:4], 0)
-        chunks_left(PS1, 1)
+        chunks_left(YC.at[0:4], 1)
 
     @pl.when(outer)
     def _():
-        chunks_left(PS1.at[0:4], 0)
         chunks_left(PS1, 1)
 
     for key, tiles in TILES.items():
         jj, t = key
-        for part, (lo, hi) in enumerate(((0, FIRST[key]), (FIRST[key], len(tiles)))):
+        for part in range(3):
+            lo, hi = ENDS[key][part : part + 2]
             for count in (1, 2):
                 if lo < hi:
 
@@ -796,7 +824,8 @@
             pltpu.VMEM((ROWS, WIDTH), BF16),
             pltpu.VMEM((ROWS, WIDTH), BF16),
             pltpu.VMEM((CHUNKS, 2 * ROWS, CW), BF16),
-            pltpu.VMEM((CHUNKS // 2, ROWS, CW), BF16),
+            pltpu.VMEM(chunks, BF16),
+            pltpu.VMEM(chunks, BF16),
             pltpu.VMEM((CHUNKS, 3 * ROWS, CW), BF16),
             pltpu.VMEM(chunks, F32),
             pltpu.VMEM((ROWS, 128), F32),
@@ -831,7 +860,7 @@
             pltpu.VMEM((8, 128), F32),
             pltpu.VMEM((8, 8, 128), F32),
             dma((6,)), dma((1,)), dma((4,)), dma((4, 4)), dma((4,)), dma((2,)), dma((8,)), dma((4,)), dma((4,)),
-            dma((2, 4)), dma((2,)), dma((1,)), dma((1,)), dma((1,)), dma((4,)), dma((1,)), dma((1,)),
+            dma((3, 4)), dma((3,)), dma((1,)), dma((1,)), dma((1,)), dma((4,)), dma((1,)), dma((1,)),
             dma((4,)), dma((4,)),
         ],
         compiler_params=pltpu.CompilerParams(

time: 68.1 us -> 62.9 us (0.924)
  the two profiles are of different devices: /device:TPU:2 before, /device:TPU:6 now
where the time goes in v4:
time: 62.9 us; the launch traced here: 62.7 us
  Pallas kernels  61 us (97%)
  local copies, waits for them, and re-layouts  1.03 us (2%)
  between operations  0.69 us (1%)
    pallas_call x1, Pallas kernels, per_device(): pl.pallas_call(kernel, out_shape=(jax.ShapeDtypeStruct((1, ROWS, WIDTH),...  59.6 us
    pallas_call x1, Pallas kernels, per_device(): pl.pallas_call(writer, out_shape=(jax.ShapeDtypeStruct((1, ROWS, WIDTH),...  1.37 us

profile of v4, /device:TPU:6, one launch (start us, length us, event | category | flops | bytes accessed | tf_op | source)
XLA Modules:
  0.0 62.7 jit_solution(16297981757085038947)
XLA Ops:
  0.6 0.0 copy-start
  0.6 0.0 copy-start.1
  0.7 0.0 copy-start.2
  0.7 1.0 %copy.15 = bf16[64,4,512]{2,0,1:T(8,128)(2,1)S(1)} copy(bf16[64,4,512]{2,1,0:T(4,128)(2,1)} %param.12) | data formatting | bytes 524288 | tf_op args[5]
  1.7 0.0 copy-done
  1.7 0.0 copy-done.1
  1.7 0.0 copy-done.2
  1.7 59.6 %span.1 = (bf16[1,128,3072]{2,1,0:T(8,128)(2,1)S(1)}, bf16[1,128,3072]{2,1,0:T(8,128)(2,1)S(1)}, f32[64,4,512]{2,1,0:T(4,128)S(1)}, f32[6,8,128]{2,1,0:T(8,128)S(1)}, f32[4,512]{1,0:T(4,128)S(1)}) custom-call(bf16[1,128,3072]{2,1,0:T(8,128)(2,1)} %gated_hbm.1, bf16[1,128,3072]{2,1,0:T(8,128)(2,1)} %values_hbm.1, bf16[1,128,3072]{2,1,0:T(8,128)(2,1)} %upstream_hbm.1, ...), custom_call_target="tpu_custom_call" | custom-call | tf_op jit(solution)/shard_map/span/pallas_call | solution.py:811
  61.4 1.4 %writer.1 = (bf16[1,128,3072]{2,1,0:T(8,128)(2,1)}, bf16[1,128,3072]{2,1,0:T(8,128)(2,1)}, f32[64,4,512]{2,1,0:T(4,128)}, f32[4,512]{1,0:T(4,128)}, f32[3,8,128]{2,1,0:T(8,128)}, /*index=5*/f32[3,8,128]{2,1,0:T(8,128)}) custom-call(bf16[1,128,3072]{2,1,0:T(8,128)(2,1)S(1)} %get-tuple-element.17.u, bf16[1,128,3072]{2,1,0:T(8,128)(2,1)S(1)} %get-tuple-element.18.v, ...), custom_call_target="tpu_custom_call" | custom-call | tf_op jit(solution)/shard_map/writer/pallas_call | solution.py:879
Async XLA Ops:
  0.6 1.0 %copy-start = (f32[3072]{0:T(1024)S(1)}, f32[3072]{0:T(1024)}, u32[]{:S(2)}) copy-start(f32[3072]{0:T(1024)} %param.10) | copy-start | bytes 36868
  0.6 1.0 %copy-start.1 = (f32[3072]{0:T(1024)S(1)}, f32[3072]{0:T(1024)}, u32[]{:S(2)}) copy-start(f32[3072]{0:T(1024)} %param.11) | copy-start | bytes 36868
  0.7 1.0 %copy-start.2 = (f32[4,512]{1,0:T(4,128)S(1)}, f32[4,512]{1,0:T(4,128)}, u32[]{:S(2)}) copy-start(f32[4,512]{1,0:T(4,128)} %bias.1) | copy-start | bytes 24580

commit v5 on v4

--- a/solution.py
+++ b/solution.py
@@ -34,10 +34,28 @@
     (1, 1): (0, 4, 6, 8),
     (1, 2): (0, 0, 2, 4),
     (1, 3): (0, 0, 2, 4),
-    (2, 2): (0, 2, 5, 8),
-    (2, 3): (0, 2, 5, 8),
+    (2, 2): (0, 2, 4, 8),
+    (2, 3): (0, 2, 4, 8),
     (3, 3): (0, 4, 4, 4),
 }
+
+
+def chain(key, k):
+    ends = ENDS[key]
+    return ((ends[0], ends[2]), (ends[2], ends[3]))[k]
+
+
+def places_of(t, k):
+    off = sum(ENDS[key][2] // 2 for key in TILES if key[1] == t) if k else 0
+    out = []
+    for key in TILES:
+        a, b = chain(key, k)
+        if key[1] == t and a < b:
+            out.append((key, (b - a) // 2, off))
+            off += (b - a) // 2
+    return out
+
+
 ORDER = {0: (0, 1, 2, 3), 1: (0, 1, 2, 3), 2: (2, 3, 0, 1), 3: (2, 3, 0, 1)}
 COLUMNS = {
     (0, 0): {g: (0, 128) for g in range(4)},
@@ -73,7 +91,7 @@
     gated_hbm, values_hbm, upstream_hbm, gain, shift, WT, bias,
     out_u, out_v, out_mix, out_vec, out_bias,
     gated, values, upstream,
-    XC, XF, XR, YC, UN, MEAN, INV, RES, YP, PS1, PS2, PSQ, PR, PQ, ACC,
+    XC, XF, XR, UR, YC, UN, MEAN, INV, RES, YP, PS1, PS2, PSQ, PR, PQ, ACC,
     WBUF, WX, WXT, BIASC, GX, GS, GR, GZ, ZR, YS, YR, ZS, ZG,
     VS, VA, VT, VB, VU, VC, VW, VD,
     in_s, w_s, f_s, w_r, w_r2, m_s, m_r, y_r, p_r, r1_s, r1_r, r2_s, r2_r, r3_s, r3_r, r4_s, r4_r,
@@ -277,6 +295,7 @@
         loop(0, CHUNKS, lambda c: norm(c, YC, 0), "norm")
 
     VS[...] = jnp.zeros_like(VS)
+    out_mix[...] = jnp.zeros_like(out_mix)
     GX[...] = jnp.zeros_like(GX)
     ACC[...] = jnp.zeros_like(ACC)
     ones = jnp.ones((8, CW), BF16)
@@ -418,51 +437,132 @@
                     def _():
                         GR[e, lo:hi] = GS[t, h, lo:hi]
 
-    def sum_dp(key, tiles):
-        n = len(tiles)
-        with jax.named_scope("r1_wait"):
-            for part in range(3):
-                a, b = ENDS[key][part : part + 2]
-                if a < b:
-                    there = GR.at[0:7, a:b]
-                    remote(there, there, r1_s.at[0, 0], r1_r.at[part], partner).wait_recv()
-
-        def add(i):
-            total = GR[0, i].astype(F32)
+    def sum_dp(k):
+        def body(key):
+            a, b = chain(key, k)
+            with jax.named_scope("r1_wait"):
+                for part in (0, 1) if k == 0 else (2,):
+                    lo, hi = ENDS[key][part : part + 2]
+                    if lo < hi:
+                        there = GR.at[0:7, lo:hi]
+                        remote(there, there, r1_s.at[0, 0], r1_r.at[part], partner).wait_recv()
+
+            def add(i):
+                total = GR[0, i].astype(F32)
+                for e in range(1, 8):
+                    total = total + GR[e, i].astype(F32)
+                total = total.astype(BF16)
+                for rs in range(4):
+                    GZ[rs, i] = total[rs * 16 : (rs + 1) * 16]
+
+            loop(a, b, add, "dp_add")
+            m = (b - a) // 2
+            at = a // 2
+
+            def piece(e):
+                return pl.ds(a + (e // 4) * m, m)
+
+            def send(o):
+                e, peer = z_peer(o)
+                remote(GZ.at[e % 4, piece(e)], ZR.at[z, at : at + m], r2_s.at[k], r2_r.at[k], peer).start()
+
+            loop(1, 8, send, "r2_send")
+            ZR[z, at : at + m] = GZ[z % 4, piece(z)]
+
+        return body
+
+    def sum_z(k):
+        def body(key):
+            a, b = chain(key, k)
+            m = (b - a) // 2
+            here = slice(a // 2, a // 2 + m)
+            with jax.named_scope("r2_wait"):
+                there = ZR.at[0:7, here]
+                remote(there, there, r2_s.at[k], r2_r.at[k], partner).wait_recv()
+            total = ZR[0, here].astype(F32)
             for e in range(1, 8):
-                total = total + GR[e, i].astype(F32)
-            total = total.astype(BF16)
-            for rs in range(4):
-                GZ[rs, i] = total[rs * 16 : (rs + 1) * 16]
-
-        loop(0, n, add, "dp_add")
-        m = n // 2
-
-        def send(o):
-            e, peer = z_peer(o)
-            remote(GZ.at[e % 4, pl.ds((e // 4) * m, m)], ZR.at[z, 0:m], r2_s.at[0], r2_r.at[0], peer).start()
-
-        loop(1, 8, send, "r2_send")
-        ZR[z, 0:m] = GZ[z % 4, pl.ds((z // 4) * m, m)]
-
-    def sum_z(key, tiles):
-        jj = key[0]
-        m = len(tiles) // 2
-
-        with jax.named_scope("r2_wait"):
-            there = ZR.at[0:7, 0:m]
-            remote(there, there, r2_s.at[0], r2_r.at[0], partner).wait_recv()
-        total = ZR[0, 0:m].astype(F32)
+                total = total + ZR[e, here].astype(F32)
+            YS[here] = total.astype(BF16)
+
+            def send(o):
+                e, peer = y_peer(o)
+                remote(YS.at[here], YR.at[y, here], r3_s.at[k], r3_r.at[k, key[0]], peer).start()
+
+            loop(1, 8, send, "r3_send")
+            YR[y, here] = YS[here]
+
+        return body
+
+    def join(k):
+        for t in range(4):
+            places = places_of(t, k)
+            if not places:
+                continue
+
+            @pl.when(x == t)
+            def _(places=places):
+                for key, m, off in places:
+                    jj = key[0]
+                    at = chain(key, k)[0] // 2
+                    for count in (1, 2):
+
+                        @pl.when((j == jj) if count == 1 else (j != jj))
+                        @jax.named_scope("r3_wait")
+                        def _():
+                            there = YR.at[0:count, at : at + m]
+                            remote(there, there, r3_s.at[k], r3_r.at[k, jj], partner).wait_recv()
+
+                    for i in range(m):
+                        ZS[off + i] = (YR[jj, at + i].astype(F32) + YR[jj + 4, at + i].astype(F32)).astype(BF16)
+                here = slice(places[0][2], places[-1][2] + places[-1][1])
+
+                def send(o):
+                    e, peer = z_peer(o)
+                    remote(ZS.at[here], ZG.at[z, here], r4_s.at[k], r4_r.at[k], peer).start()
+
+                loop(1, 8, send, "r4_send")
+                ZG[z, here] = ZS[here]
+
+    def put_mix(k):
+        keep = lax.broadcasted_iota(jnp.int32, (16, 128), 1) // 64 <= core
+        for t in range(4):
+            places = places_of(t, k)
+            if not places:
+                continue
+
+            @pl.when(x == t)
+            def _(t=t, places=places):
+                there = ZG.at[0:7, places[0][2] : places[-1][2] + places[-1][1]]
+                with jax.named_scope("r4_wait"):
+                    remote(there, there, r4_s.at[k], r4_r.at[k], partner).wait()
+                for part in range(8):
+                    rows = slice(16 * (part % 4), 16 * (part % 4) + 16)
+                    for key, m, off in places:
+                        for i in range(m):
+                            s, g = TILES[key][chain(key, k)[0] + (part // 4) * m + i]
+                            value = ZG[part, off + i].astype(F32)
+                            if s == t:
+                                value = jnp.where(keep, value, 0.0)
+                            out_mix[rows, g, s * 128 : (s + 1) * 128] = value
+
+    def vec_send(source, land, me, k, peer):
+        for o in range(1, 8):
+            e, to = peer(o)
+            remote(source(e), land.at[me], v_s.at[k], v_r.at[k], to).start()
+
+    def vec_wait(land, k):
+        with jax.named_scope("v_wait"):
+            remote(land.at[0:7], land.at[0:7], v_s.at[k], v_r.at[k], partner).wait()
+
+    def vec_sum(land):
+        total = land[0]
         for e in range(1, 8):
-            total = total + ZR[e, 0:m].astype(F32)
-        YS[0:m] = total.astype(BF16)
-
-        def send(o):
-            e, peer = y_peer(o)
-            remote(YS.at[0:m], YR.at[y, 0:m], r3_s.at[0], r3_r.at[jj], peer).start()
-
-        loop(1, 8, send, "r3_send")
-        YR[y, 0:m] = YS[0:m]
+            total = total + land[e]
+        return total
+
+    def vec_dp():
+        vec_send(lambda e: VS.at[e], VA, d, 0, dp_peer)
+        VA[d] = VS[d]
 
     @pl.when(inner)
     def _():
@@ -505,38 +605,52 @@
             def _():
                 outer_sums(c)
 
-        def second(c):
+        def meet(c):
             g = c // 2
             with jax.named_scope("wait_x"):
                 arrived(c)
             take(c)
+            with jax.named_scope("wait_y"):
+                both_y = YC.at[c, pl.ds(ROWS, 2 * ROWS), :]
+                remote(both_y, both_y, m_s.at[0], y_r.at[c % 4], opp_inner).wait_recv()
+
+            @pl.when(upper)
+            def _():
+                raw = YC[c, pl.ds(ROWS, 2 * ROWS), :]
+                UR[c % 4] = raw
+                n = raw.astype(F32) * gain[:, columns(c)] + shift[:, columns(c)]
+                YC[c, pl.ds(ROWS, 2 * ROWS), :] = n.astype(BF16)
+
+            GX[g] += dot_t(YC[c], XC[c])
+
+        def multiply(c, now):
+            g = c // 2
             r = dot(WX[g], XC[c])
             PS1[c] = r[ROWS : 2 * ROWS].astype(BF16)
             PS2[c] = r[2 * ROWS :].astype(BF16)
-            p_outer(c).start()
-            p_inner(c).start()
+            if now:
+                p_outer(c).start()
+                p_inner(c).start()
             put_x(c, g, r[0:ROWS])
-            with jax.named_scope("wait_y"):
-                both_y = YC.at[c, pl.ds(ROWS, 2 * ROWS), :]
-                remote(both_y, both_y, m_s.at[0], y_r.at[c % 4], opp_inner).wait_recv()
-
-            @pl.when(upper)
-            def _():
-                u = YC[c, pl.ds(ROWS, 2 * ROWS), :].astype(F32)
-                near, far = PS1[c].astype(F32), PS2[c].astype(F32)
-                column_sums(c, near * u[0:ROWS] + far * u[ROWS:], near + far)
-                YC[c, pl.ds(ROWS, 2 * ROWS), :] = (u * gain[:, columns(c)] + shift[:, columns(c)]).astype(BF16)
-
             s = dot(WXT[g], YC[c])
             PSQ[c] = s[0:ROWS].astype(BF16)
             put_y(c, g, s[ROWS:], True)
             q_outer(c).start()
-            GX[g] += dot_t(YC[c], XC[c])
 
             @pl.when(lower)
             def _():
                 outer_sums(c)
 
+            @pl.when(upper)
+            def _():
+                u = UR[c % 4].astype(F32)
+                near, far = PS1[c].astype(F32), PS2[c].astype(F32)
+                column_sums(c, near * u[0:ROWS] + far * u[ROWS:], near + far)
+
+        def second(c):
+            meet(c)
+            multiply(c, True)
+
         for i in range(4):
             for jj in (1, 2):
 
@@ -546,11 +660,17 @@
 
             if i < 2:
                 loop(2 * i, 2 * i + 2, lambda q: first(phys(q)), "first")
+            elif i == 2:
+                loop(2 * i, 2 * i + 2, lambda q: second(phys(q)), "second")
             else:
-                loop(2 * i, 2 * i + 2, lambda q: second(phys(q)), "second")
+                loop(2 * i, 2 * i + 2, lambda q: meet(phys(q)), "meet")
             if i > 0:
                 with jax.named_scope("stage"):
                     stage(i - 1)
+        with jax.named_scope("multiply"):
+            multiply(phys(6), True)
+            multiply(phys(7), False)
+        vec_dp()
 
     @pl.when(outer)
     def _():
@@ -594,31 +714,12 @@
         put_y(c, c // 2, YP[c] + PQ[c].astype(F32), False)
 
     def owned(places, body):
-        for key, tiles in TILES.items():
+        for key in TILES:
             if key[0] in places:
 
                 @pl.when((j == key[0]) & (x == key[1]))
-                def _(key=key, tiles=tiles):
-                    body(key, tiles)
-
-    def vec_send(source, land, me, k, peer):
-        for o in range(1, 8):
-            e, to = peer(o)
-            remote(source(e), land.at[me], v_s.at[k], v_r.at[k], to).start()
-
-    def vec_wait(land, k):
-        with jax.named_scope("v_wait"):
-            remote(land.at[0:7], land.at[0:7], v_s.at[k], v_r.at[k], partner).wait()
-
-    def vec_sum(land):
-        total = land[0]
-        for e in range(1, 8):
-            total = total + land[e]
-        return total
-
-    def vec_dp():
-        vec_send(lambda e: VS.at[e], VA, d, 0, dp_peer)
-        VA[d] = VS[d]
+                def _(key=key):
+                    body(key)
 
     def vec_z():
         vec_wait(VA, 0)
@@ -634,33 +735,38 @@
 
     @pl.when(inner)
     def _():
+        owned((1, 2), sum_dp(0))
+        vec_z()
+        owned((1, 2), sum_dp(1))
+        loop(0, 2, late, "late")
+        owned((1, 2), sum_z(0))
+        p_outer(phys(7)).start()
+        p_inner(phys(7)).start()
+        vec_y()
+        owned((1, 2), sum_z(1))
+
+    @pl.when(outer)
+    def _():
         vec_dp()
-        late(0)
-        vec_z()
-        late(1)
-        owned((1, 2), sum_dp)
-        vec_y()
-        late(2)
-        owned((1, 2), sum_z)
-
-    @pl.when(outer)
-    def _():
-        vec_dp()
-        owned((0, 3), sum_dp)
+        owned((0, 3), sum_dp(0))
         loop(0, 4, near_part, "near_part")
-        owned((0, 3), sum_z)
+        owned((0, 3), sum_z(0))
         vec_z()
         loop(4, 6, near_whole, "near_whole")
         vec_y()
         loop(6, 8, near_whole, "near_whole")
-        loop(0, 3, late, "late")
-
+        loop(0, 2, late, "late")
+
+    join(0)
+    with jax.named_scope("late"):
+        late(2)
+    with jax.named_scope("late"):
+        late(3)
     vec_wait(VC, 2)
     VW[...] = vec_sum(VC)
     vec_send(lambda e: VW, VD, d, 3, dp_peer)
     VD[d] = VW[...]
-    with jax.named_scope("late"):
-        late(3)
+    join(1)
 
     mean_a = jnp.sum(ACC[0], axis=1, keepdims=True) * (1.0 / WIDTH)
     mean_b = jnp.sum(ACC[1], axis=1, keepdims=True) * (1.0 / WIDTH)
@@ -674,34 +780,6 @@
         out_u[0, :, cols] = (upstream[:, cols].astype(F32) * RES[0, c].astype(F32)).astype(BF16)
 
     loop(0, CHUNKS, outputs, "outputs")
-
-    for t in range(4):
-        places = [(jj, tiles) for (jj, tt), tiles in TILES.items() if tt == t]
-        total_tiles = sum(len(tiles) // 2 for _, tiles in places)
-
-        @pl.when(x == t)
-        def _(t=t, places=places, total_tiles=total_tiles):
-            off = 0
-            for jj, tiles in places:
-                m = len(tiles) // 2
-                for count in (1, 2):
-
-                    @pl.when((j == jj) if count == 1 else (j != jj))
-                    @jax.named_scope("r3_wait")
-                    def _():
-                        there = YR.at[0:count, 0:m]
-                        remote(there, there, r3_s.at[0], r3_r.at[jj], partner).wait_recv()
-
-                for i in range(m):
-                    ZS[off + i] = (YR[jj, i].astype(F32) + YR[jj + 4, i].astype(F32)).astype(BF16)
-                off += m
-
-            def send(o):
-                e, peer = z_peer(o)
-                remote(ZS.at[0:total_tiles], ZG.at[z, 0:total_tiles], r4_s.at[0], r4_r.at[0], peer).start()
-
-            loop(1, 8, send, "r4_send")
-            ZG[z, 0:total_tiles] = ZS[0:total_tiles]
 
     for key in COLUMNS:
 
@@ -743,39 +821,17 @@
                         there = GS.at[0, 0:count, lo:hi]
                         remote(there, there, r1_s.at[part, t], r1_r.at[part], partner).wait_send()
 
-    def sent(key, tiles):
-        m = len(tiles) // 2
-
-        there = ZR.at[0:7, 0:m]
-        remote(there, there, r2_s.at[0], r2_r.at[0], partner).wait_send()
-        remote(there, there, r3_s.at[0], r3_r.at[0], partner).wait_send()
+    def sent(key):
+        for k in range(2):
+            a, b = chain(key, k)
+            if a < b:
+                there = ZR.at[0:7, 0 : (b - a) // 2]
+                remote(there, there, r2_s.at[k], r2_r.at[k], partner).wait_send()
+                remote(there, there, r3_s.at[k], r3_r.at[k, 0], partner).wait_send()
 
     owned((0, 1, 2, 3), sent)
-
-    out_mix[...] = jnp.zeros_like(out_mix)
-    keep = lax.broadcasted_iota(jnp.int32, (16, 128), 1) // 64 <= core
-    for t in range(4):
-        places = [(jj, tiles) for (jj, tt), tiles in TILES.items() if tt == t]
-        total_tiles = sum(len(tiles) // 2 for _, tiles in places)
-
-        @pl.when(x == t)
-        def _(t=t, places=places, total_tiles=total_tiles):
-            with jax.named_scope("r4_wait"):
-                there = ZG.at[0:7, 0:total_tiles]
-                remote(there, there, r4_s.at[0], r4_r.at[0], partner).wait()
-            for k in range(8):
-                rows = slice(16 * (k % 4), 16 * (k % 4) + 16)
-                off = 0
-                for jj, tiles in places:
-                    m = len(tiles) // 2
-                    for i in range(m):
-                        s, g = tiles[(k // 4) * m + i]
-                        value = ZG[k, off + i].astype(F32)
-                        if s == t:
-                            value = jnp.where(keep, value, 0.0)
-                        out_mix[rows, g, s * 128 : (s + 1) * 128] = value
-                    off += m
-
+    put_mix(0)
+    put_mix(1)
     vec_wait(VD, 3)
     out_vec[...] = VD[0:6]
     for g in range(GROUPS):
@@ -826,6 +882,7 @@
             pltpu.VMEM((CHUNKS, 2 * ROWS, CW), BF16),
             pltpu.VMEM(chunks, BF16),
             pltpu.VMEM(chunks, BF16),
+            pltpu.VMEM((CHUNKS // 2, 2 * ROWS, CW), BF16),
             pltpu.VMEM((CHUNKS, 3 * ROWS, CW), BF16),
             pltpu.VMEM(chunks, F32),
             pltpu.VMEM((ROWS, 128), F32),
@@ -860,7 +917,7 @@
             pltpu.VMEM((8, 128), F32),
             pltpu.VMEM((8, 8, 128), F32),
             dma((6,)), dma((1,)), dma((4,)), dma((4, 4)), dma((4,)), dma((2,)), dma((8,)), dma((4,)), dma((4,)),
-            dma((3, 4)), dma((3,)), dma((1,)), dma((1,)), dma((1,)), dma((4,)), dma((1,)), dma((1,)),
+            dma((3, 4)), dma((3,)), dma((2,)), dma((2,)), dma((2,)), dma((2, 4)), dma((2,)), dma((2,)),
             dma((4,)), dma((4,)),
         ],
         compiler_params=pltpu.CompilerParams(

time: 62.9 us -> 60.8 us (0.967)
  the two profiles are of different devices: /device:TPU:6 before, /device:TPU:1 now
where the time goes in v5:
time: 60.8 us; the launch traced here: 60.2 us
  Pallas kernels  58.5 us (96%)
  local copies, waits for them, and re-layouts  1.03 us (2%)
  between operations  0.69 us (1%)
    pallas_call x1, Pallas kernels, per_device(): pl.pallas_call(kernel, out_shape=(jax.ShapeDtypeStruct((1, ROWS, WIDTH),...  57.1 us
    pallas_call x1, Pallas kernels, per_device(): pl.pallas_call(writer, out_shape=(jax.ShapeDtypeStruct((1, ROWS, WIDTH),...  1.37 us

profile of v5, /device:TPU:1, one launch (start us, length us, event | category | flops | bytes accessed | tf_op | source)
XLA Modules:
  0.0 60.2 jit_solution(6582592959440039959)
XLA Ops:
  0.6 0.0 copy-start
  0.6 0.0 copy-start.1
  0.7 0.0 copy-start.2
  0.7 1.0 %copy.15 = bf16[64,4,512]{2,0,1:T(8,128)(2,1)S(1)} copy(bf16[64,4,512]{2,1,0:T(4,128)(2,1)} %param.12) | data formatting | bytes 524288 | tf_op args[5]
  1.7 0.0 copy-done
  1.7 0.0 copy-done.1
  1.7 0.0 copy-done.2
  1.7 57.1 %span.1 = (bf16[1,128,3072]{2,1,0:T(8,128)(2,1)S(1)}, bf16[1,128,3072]{2,1,0:T(8,128)(2,1)S(1)}, f32[64,4,512]{2,1,0:T(4,128)S(1)}, f32[6,8,128]{2,1,0:T(8,128)S(1)}, f32[4,512]{1,0:T(4,128)S(1)}) custom-call(bf16[1,128,3072]{2,1,0:T(8,128)(2,1)} %gated_hbm.1, bf16[1,128,3072]{2,1,0:T(8,128)(2,1)} %values_hbm.1, bf16[1,128,3072]{2,1,0:T(8,128)(2,1)} %upstream_hbm.1, ...), custom_call_target="tpu_custom_call" | custom-call | tf_op jit(solution)/shard_map/span/pallas_call | solution.py:867
  58.8 1.4 %writer.1 = (bf16[1,128,3072]{2,1,0:T(8,128)(2,1)}, bf16[1,128,3072]{2,1,0:T(8,128)(2,1)}, f32[64,4,512]{2,1,0:T(4,128)}, f32[4,512]{1,0:T(4,128)}, f32[3,8,128]{2,1,0:T(8,128)}, /*index=5*/f32[3,8,128]{2,1,0:T(8,128)}) custom-call(bf16[1,128,3072]{2,1,0:T(8,128)(2,1)S(1)} %get-tuple-element.17.u, bf16[1,128,3072]{2,1,0:T(8,128)(2,1)S(1)} %get-tuple-element.18.v, ...), custom_call_target="tpu_custom_call" | custom-call | tf_op jit(solution)/shard_map/writer/pallas_call | solution.py:936
Async XLA Ops:
  0.6 1.0 %copy-start = (f32[3072]{0:T(1024)S(1)}, f32[3072]{0:T(1024)}, u32[]{:S(2)}) copy-start(f32[3072]{0:T(1024)} %param.10) | copy-start | bytes 36868
  0.6 1.0 %copy-start.1 = (f32[3072]{0:T(1024)S(1)}, f32[3072]{0:T(1024)}, u32[]{:S(2)}) copy-start(f32[3072]{0:T(1024)} %param.11) | copy-start | bytes 36868
  0.7 1.0 %copy-start.2 = (f32[4,512]{1,0:T(4,128)S(1)}, f32[4,512]{1,0:T(4,128)}, u32[]{:S(2)}) copy-start(f32[4,512]{1,0:T(4,128)} %bias.1) | copy-start | bytes 24580

commit v6 on v5

--- a/solution.py
+++ b/solution.py
@@ -85,6 +85,14 @@
 def loop(lo, hi, body, name="loop"):
     with jax.named_scope(name):
         lax.fori_loop(lo, hi, lambda i, _: (body(i), None)[1], None)
+
+
+FAR_FIRST = (4, 3, 5, 2, 6, 1, 7)
+
+
+def far_first(body):
+    for o in FAR_FIRST:
+        body(o)
 
 
 def kernel(
@@ -466,7 +474,7 @@
                 e, peer = z_peer(o)
                 remote(GZ.at[e % 4, piece(e)], ZR.at[z, at : at + m], r2_s.at[k], r2_r.at[k], peer).start()
 
-            loop(1, 8, send, "r2_send")
+            far_first(send)
             ZR[z, at : at + m] = GZ[z % 4, piece(z)]
 
         return body
@@ -488,7 +496,7 @@
                 e, peer = y_peer(o)
                 remote(YS.at[here], YR.at[y, here], r3_s.at[k], r3_r.at[k, key[0]], peer).start()
 
-            loop(1, 8, send, "r3_send")
+            far_first(send)
             YR[y, here] = YS[here]
 
         return body
@@ -520,7 +528,7 @@
                     e, peer = z_peer(o)
                     remote(ZS.at[here], ZG.at[z, here], r4_s.at[k], r4_r.at[k], peer).start()
 
-                loop(1, 8, send, "r4_send")
+                far_first(send)
                 ZG[z, here] = ZS[here]
 
     def put_mix(k):
@@ -546,7 +554,7 @@
                             out_mix[rows, g, s * 128 : (s + 1) * 128] = value
 
     def vec_send(source, land, me, k, peer):
-        for o in range(1, 8):
+        for o in FAR_FIRST:
             e, to = peer(o)
             remote(source(e), land.at[me], v_s.at[k], v_r.at[k], to).start()
 
@@ -736,8 +744,8 @@
     @pl.when(inner)
     def _():
         owned((1, 2), sum_dp(0))
+        owned((1, 2), sum_dp(1))
         vec_z()
-        owned((1, 2), sum_dp(1))
         loop(0, 2, late, "late")
         owned((1, 2), sum_z(0))
         p_outer(phys(7)).start()
@@ -831,12 +839,12 @@
 
     owned((0, 1, 2, 3), sent)
     put_mix(0)
-    put_mix(1)
     vec_wait(VD, 3)
     out_vec[...] = VD[0:6]
     for g in range(GROUPS):
         for k in range(4):
             out_bias[g : g + 1, k * 128 : (k + 1) * 128] = VD[6 + g // 2, (g % 2) * 4 + k : (g % 2) * 4 + k + 1]
+    put_mix(1)
 
 
 def writer(u, v, mix, vec, bias, out_u, out_v, out_mix, out_bias, out_gain, out_shift, sems):

time: 60.8 us -> 60.6 us (level)
  no operation moved by 1% of the time
where the time goes in v6:
time: 60.6 us; the launch traced here: 60.1 us
  Pallas kernels  58.4 us (96%)
  local copies, waits for them, and re-layouts  1.03 us (2%)
  between operations  0.69 us (1%)
    pallas_call x1, Pallas kernels, per_device(): pl.pallas_call(kernel, out_shape=(jax.ShapeDtypeStruct((1, ROWS, WIDTH),...  57 us
    pallas_call x1, Pallas kernels, per_device(): pl.pallas_call(writer, out_shape=(jax.ShapeDtypeStruct((1, ROWS, WIDTH),...  1.37 us

profile of v6, /device:TPU:1, one launch (start us, length us, event | category | flops | bytes accessed | tf_op | source)
XLA Modules:
  0.0 60.1 jit_solution(3351654761001374509)
XLA Ops:
  0.6 0.0 copy-start
  0.6 0.0 copy-start.1
  0.7 0.0 copy-start.2
  0.7 1.0 %copy.15 = bf16[64,4,512]{2,0,1:T(8,128)(2,1)S(1)} copy(bf16[64,4,512]{2,1,0:T(4,128)(2,1)} %param.12) | data formatting | bytes 524288 | tf_op args[5]
  1.7 0.0 copy-done
  1.7 0.0 copy-done.1
  1.7 0.0 copy-done.2
  1.7 57.0 %span.1 = (bf16[1,128,3072]{2,1,0:T(8,128)(2,1)S(1)}, bf16[1,128,3072]{2,1,0:T(8,128)(2,1)S(1)}, f32[64,4,512]{2,1,0:T(4,128)S(1)}, f32[6,8,128]{2,1,0:T(8,128)S(1)}, f32[4,512]{1,0:T(4,128)S(1)}) custom-call(bf16[1,128,3072]{2,1,0:T(8,128)(2,1)} %gated_hbm.1, bf16[1,128,3072]{2,1,0:T(8,128)(2,1)} %values_hbm.1, bf16[1,128,3072]{2,1,0:T(8,128)(2,1)} %upstream_hbm.1, ...), custom_call_target="tpu_custom_call" | custom-call | tf_op jit(solution)/shard_map/span/pallas_call | solution.py:875
  58.7 1.4 %writer.1 = (bf16[1,128,3072]{2,1,0:T(8,128)(2,1)}, bf16[1,128,3072]{2,1,0:T(8,128)(2,1)}, f32[64,4,512]{2,1,0:T(4,128)}, f32[4,512]{1,0:T(4,128)}, f32[3,8,128]{2,1,0:T(8,128)}, /*index=5*/f32[3,8,128]{2,1,0:T(8,128)}) custom-call(bf16[1,128,3072]{2,1,0:T(8,128)(2,1)S(1)} %get-tuple-element.17.u, bf16[1,128,3072]{2,1,0:T(8,128)(2,1)S(1)} %get-tuple-element.18.v, ...), custom_call_target="tpu_custom_call" | custom-call | tf_op jit(solution)/shard_map/writer/pallas_call | solution.py:944
Async XLA Ops:
  0.6 1.0 %copy-start = (f32[3072]{0:T(1024)S(1)}, f32[3072]{0:T(1024)}, u32[]{:S(2)}) copy-start(f32[3072]{0:T(1024)} %param.10) | copy-start | bytes 36868
  0.6 1.0 %copy-start.1 = (f32[3072]{0:T(1024)S(1)}, f32[3072]{0:T(1024)}, u32[]{:S(2)}) copy-start(f32[3072]{0:T(1024)} %param.11) | copy-start | bytes 36868
  0.7 1.0 %copy-start.2 = (f32[4,512]{1,0:T(4,128)S(1)}, f32[4,512]{1,0:T(4,128)}, u32[]{:S(2)}) copy-start(f32[4,512]{1,0:T(4,128)} %bias.1) | copy-start | bytes 24580
